TPU v7x, 32 devices: a whole 2x2x4 slice. The times are simulated.
32 devices in a mesh: sp: 8 (over z, y), dp: 4 (over x, core).
Axes of the slice: x: 2, y: 2, z: 4, core: 2. Of those that a mesh axis runs over, the one named last changes fastest.
Arguments:
- residual: bfloat16 [4, 1024, 2048], P('dp', 'sp'), may hold values from -6 to 6
- head_input: bfloat16 [4, 1024, 2048], P('dp', 'sp'), may hold values from -6 to 6
- gate_input: bfloat16 [4, 1024, 2048], P('dp', 'sp'), may hold values from -6 to 6
- b_input: bfloat16 [4, 1024, 1024], P('dp', 'sp'), may hold values from -6 to 6
- c_input: bfloat16 [4, 1024, 1024], P('dp', 'sp'), may hold values from -6 to 6
- step_input: bfloat16 [4, 1024, 32], P('dp', 'sp'), may hold values from -4.8 to 4.8
- conv_weight: bfloat16 [4, 2048], replicated, may hold values from -3 to 3
- conv_b_weight: bfloat16 [4, 1024], replicated, may hold values from -3 to 3
- conv_c_weight: bfloat16 [4, 1024], replicated, may hold values from -3 to 3
- step_bias: float32 [32], replicated, may hold values from -1 to 1
- decay_log: float32 [32], replicated, may hold values from -9.92 to -2.99
- skip: float32 [32], replicated, may hold values from 0.5 to 1.5
- norm_gain: float32 [2048], replicated, may hold values from 0.1 to 1.9
- out_weight: bfloat16 [2048, 2048], P('dp'), may hold values from -0.125 to 0.125
- ffn_gain: float32 [2048], replicated, may hold values from 0.1 to 1.9
- shared_gate: bfloat16 [2048, 512], replicated, may hold values from -0.125 to 0.125
- shared_up: bfloat16 [2048, 512], replicated, may hold values from -0.125 to 0.125
- shared_down: bfloat16 [512, 2048], replicated, may hold values from -0.25 to 0.25
- expert_gate: bfloat16 [32, 2048, 512], P(('sp', 'dp')), may hold values from -0.125 to 0.125
- expert_up: bfloat16 [32, 2048, 512], P(('sp', 'dp')), may hold values from -0.125 to 0.125
- expert_down: bfloat16 [32, 512, 2048], P(('sp', 'dp')), may hold values from -0.25 to 0.25
- routes: int32 [4, 1024, 2], P('dp', 'sp'), may hold values from 0 to 31, all different within a row; in each aligned block of 128 rows (0 to 127, 128 to 255, ..., all dimensions but the last counted through in order) at most 16 rows name the same one
- route_weights: float32 [4, 1024, 2], P('dp', 'sp'), may hold values from 0.25 to 1.25
Outputs:
- layer_out: bfloat16 [4, 1024, 2048], P('dp', 'sp')
Inputs may be any that keep to these rules, and one draw needn't show every extreme that they name: `routes`: each token names 2 different experts; among the rows of one device no expert is named more than 16 times, a bound that some block reaches.
All inputs are finite; a program needn't handle non-finite values.
Results may differ from a plain program's by a relative error of at most 0.015.
Values may be sent and summed in bfloat16 or wider, within the bound.
A program may use at most 128 MiB of HBM per device.

v0:
```python
import jax
import jax.numpy as jnp
from jax import lax
from jax.experimental import pallas as pl
from jax.experimental.pallas import tpu as pltpu
from jax.sharding import PartitionSpec as P

EPS = 1e-06
HIGH = lax.Precision.HIGHEST
HALO = 8
TAIL = 16
F32 = jnp.float32
BF16 = jnp.bfloat16


def silu(v):
    return v * (1.0 / (1.0 + jnp.exp(-v)))


def conv_silu(halo, rows, taps):
    count = taps.shape[0]
    length = rows.shape[0]
    padded = jnp.concatenate([halo.astype(F32), rows.astype(F32)], axis=0)
    total = None
    for tap in range(count):
        start = HALO - (count - 1) + tap
        term = padded[start : start + length] * taps[tap : tap + 1].astype(F32)
        total = term if total is None else total + term
    return silu(total)


def spread(columns, first, count, width):
    rows = columns.shape[0]
    return jnp.concatenate(
        [jnp.broadcast_to(columns[:, first + j : first + j + 1], (rows, width)) for j in range(count)],
        axis=1,
    )


def block_kernel(
    x_ref, b_ref, c_ref, halo_ref, step_ref, wx_ref, wb_ref, wc_ref, bias_ref, log_ref, skip_ref,
    y_ref, cm_ref, grow_ref, state_ref, *, groups, local,
):
    length, inner = x_ref.shape
    heads = step_ref.shape[1]
    span = b_ref.shape[1]
    per = heads // groups
    width = inner // heads
    state = span // groups
    wide = per * width
    raw = step_ref[...].astype(F32) + bias_ref[...]
    step = jnp.maximum(raw, 0.0) + jnp.log(1.0 + jnp.exp(-jnp.abs(raw)))
    logs = step * -jnp.exp(log_ref[...])
    row = lax.broadcasted_iota(jnp.int32, (length, length), 0)
    col = lax.broadcasted_iota(jnp.int32, (length, length), 1)
    lower = row >= col
    tril = lower.astype(F32)
    cum = lax.dot_general(tril, logs, (((1,), (0,)), ((), ())), precision=HIGH, preferred_element_type=F32)
    cum_t = lax.dot_general(logs, tril, (((0,), (1,)), ((), ())), precision=HIGH, preferred_element_type=F32)
    grow_ref[...] = cum
    to_end = jnp.exp(cum[length - 1 : length] - cum)
    for g in range(groups):
        xcol = slice(g * wide, (g + 1) * wide)
        bcol = slice(g * state, (g + 1) * state)
        xs = conv_silu(halo_ref[:, xcol], x_ref[:, xcol], wx_ref[:, xcol])
        bm = conv_silu(
            halo_ref[:, inner + g * state : inner + (g + 1) * state], b_ref[:, bcol], wb_ref[:, bcol]
        ).astype(BF16)
        cm = conv_silu(
            halo_ref[:, inner + span + g * state : inner + span + (g + 1) * state],
            c_ref[:, bcol], wc_ref[:, bcol],
        ).astype(BF16)
        cm_ref[:, bcol] = cm
        weighted = xs * spread(step, g * per, per, width)
        scores = lax.dot_general(cm, bm, (((1,), (1,)), ((), ())), preferred_element_type=F32)
        scores = jnp.where(lower, scores, 0.0)
        parts = []
        small = weighted.astype(BF16)
        for j in range(per):
            h = g * per + j
            decay = jnp.exp(jnp.minimum(cum[:, h : h + 1] - cum_t[h : h + 1, :], 0.0))
            parts.append(
                jnp.dot((scores * decay).astype(BF16), small[:, j * width : (j + 1) * width],
                        preferred_element_type=F32)
            )
        y_ref[:, xcol] = jnp.concatenate(parts, axis=1) + skip_ref[:, xcol] * xs
        ended = (weighted * spread(to_end, g * per, per, width)).astype(BF16)
        fresh = lax.dot_general(
            ended, bm, (((0,), (0,)), ((), ())), preferred_element_type=F32
        ).astype(BF16)
        for j in range(per):
            h = g * per + j
            at = h % local * width
            state_ref[h // local, at : at + width, :] = fresh[j * width : (j + 1) * width]
    last = cum[length - 1 : length]
    high = last.astype(BF16)
    rest = last - high.astype(F32)
    middle = rest.astype(BF16)
    low = (rest - middle.astype(F32)).astype(BF16)
    for w in range(heads // local):
        mine = slice(w * local, (w + 1) * local)
        parts = [p.astype(F32)[:, mine] for p in (high, middle, low)]
        rows = jnp.concatenate(parts + [jnp.zeros((TAIL - 3, local), F32)], axis=0)
        rows = jnp.concatenate([rows, jnp.zeros((TAIL, state - local), F32)], axis=1)
        state_ref[w, local * width :, :] = rows.astype(BF16)


def prefix_kernel(got_ref, out_ref, *, local):
    ways, rows, state = out_ref.shape
    width = rows // local
    factors = []
    for i in range(ways - 1):
        tail = got_ref[i, rows : rows + TAIL, :].astype(F32)
        factors.append(jnp.exp(tail[0:1] + tail[1:2] + tail[2:3]))
    for j in range(local):
        at = slice(j * width, (j + 1) * width)
        carry = jnp.zeros((width, state), F32)
        for i in range(ways):
            out_ref[i, at, :] = carry.astype(BF16)
            if i < ways - 1:
                factor = jnp.broadcast_to(factors[i][:, j : j + 1], (1, state))
                carry = carry * factor + got_ref[i, at, :].astype(F32)


def norm_kernel(y_ref, cm_ref, grow_ref, before_ref, gate_ref, gain_ref, out_ref, *, groups):
    length, inner = y_ref.shape
    heads = grow_ref.shape[1]
    state = before_ref.shape[1]
    per = heads // groups
    width = inner // heads
    wide = per * width
    grow = jnp.exp(grow_ref[...])
    for g in range(groups):
        xcol = slice(g * wide, (g + 1) * wide)
        outer = lax.dot_general(
            cm_ref[:, g * state : (g + 1) * state], before_ref[xcol, :],
            (((1,), (1,)), ((), ())), preferred_element_type=F32,
        )
        v = y_ref[:, xcol] + outer * spread(grow, g * per, per, width)
        v = v * silu(gate_ref[:, xcol].astype(F32))
        v = v * lax.rsqrt(jnp.mean(v * v, axis=1, keepdims=True) + EPS)
        out_ref[:, xcol] = (v * gain_ref[:, xcol]).astype(BF16)


def vmem(count):
    return [pl.BlockSpec(memory_space=pltpu.VMEM)] * count


PARAMS = pltpu.CompilerParams(vmem_limit_bytes=32 * 1024 * 1024)


def body(
    residual, head_input, gate_input, b_input, c_input, step_input, conv_weight, conv_b_weight,
    conv_c_weight, step_bias, decay_log, skip, norm_gain, out_weight, ffn_gain, shared_gate,
    shared_up, shared_down, expert_gate, expert_up, expert_down, routes, route_weights,
):
    tokens, inner = head_input.shape[1:]
    heads = step_bias.shape[0]
    state = 128
    span = b_input.shape[2]
    groups = span // state
    width = inner // heads
    model = residual.shape[2]
    ways = lax.axis_size("sp")
    local = heads // ways
    x_rows, b_rows, c_rows = head_input[0], b_input[0], c_input[0]
    weight = lax.all_gather(out_weight, "dp", axis=0, tiled=True)
    tail = jnp.concatenate([x_rows[-HALO:], b_rows[-HALO:], c_rows[-HALO:]], axis=1)
    halo = lax.ppermute(tail, "sp", [(i, i + 1) for i in range(ways - 1)])
    y, cm, cum, states = pl.pallas_call(
        lambda *refs: block_kernel(*refs, groups=groups, local=local),
        out_shape=(
            jax.ShapeDtypeStruct((tokens, inner), F32),
            jax.ShapeDtypeStruct((tokens, span), BF16),
            jax.ShapeDtypeStruct((tokens, heads), F32),
            jax.ShapeDtypeStruct((ways, local * width + TAIL, state), BF16),
        ),
        in_specs=vmem(11),
        out_specs=tuple(vmem(4)),
        compiler_params=PARAMS,
        cost_estimate=pl.CostEstimate(flops=400_000_000, bytes_accessed=5_000_000, transcendentals=1_500_000),
    )(
        x_rows, b_rows, c_rows, halo, step_input[0], conv_weight, conv_b_weight, conv_c_weight,
        step_bias[None], decay_log[None], jnp.repeat(skip, width)[None],
    )
    arrived = lax.all_to_all(states, "sp", split_axis=0, concat_axis=0, tiled=True)
    prefix = pl.pallas_call(
        lambda *refs: prefix_kernel(*refs, local=local),
        out_shape=jax.ShapeDtypeStruct((ways, local * width, state), BF16),
        in_specs=vmem(1),
        out_specs=vmem(1)[0],
        compiler_params=PARAMS,
        cost_estimate=pl.CostEstimate(flops=2_000_000, bytes_accessed=1_000_000, transcendentals=1000),
    )(arrived)
    before = lax.all_to_all(prefix, "sp", split_axis=0, concat_axis=0, tiled=True).reshape(inner, state)
    normed = pl.pallas_call(
        lambda *refs: norm_kernel(*refs, groups=groups),
        out_shape=jax.ShapeDtypeStruct((tokens, inner), BF16),
        in_specs=vmem(6),
        out_specs=vmem(1)[0],
        compiler_params=PARAMS,
        cost_estimate=pl.CostEstimate(flops=100_000_000, bytes_accessed=3_000_000, transcendentals=400_000),
    )(y, cm, cum, before, gate_input[0], norm_gain[None])

    mixed = (residual[0].astype(F32) + jnp.dot(normed, weight, preferred_element_type=F32)).astype(BF16)
    mixed_f = mixed.astype(F32)
    expert_in = (
        mixed_f * lax.rsqrt(jnp.mean(mixed_f * mixed_f, axis=1, keepdims=True) + EPS) * ffn_gain[None, :]
    ).astype(BF16)

    picks = routes.shape[2]
    ranks = ways * lax.axis_size("dp")
    experts = ranks * expert_gate.shape[0]
    slots = 2 * tokens * picks // experts
    chosen = routes[0].reshape(-1)
    pairs = chosen.shape[0]
    onehot = (chosen[:, None] == jnp.arange(experts, dtype=jnp.int32)[None, :]).astype(BF16)
    earlier = (jnp.arange(pairs)[:, None] > jnp.arange(pairs)[None, :]).astype(BF16)
    counts = jnp.dot(earlier, onehot, preferred_element_type=F32)
    position = jnp.sum(counts * onehot.astype(F32), axis=1).astype(jnp.int32)
    target = (chosen * slots + position).reshape(tokens, picks)
    lanes = jnp.arange(experts * slots, dtype=jnp.int32)
    combine = jnp.zeros((tokens, experts * slots), F32)
    choose = jnp.zeros((experts * slots, tokens), BF16)
    for k in range(picks):
        combine = combine + jnp.where(target[:, k, None] == lanes[None, :], route_weights[0][:, k, None], 0.0)
        choose = choose + (lanes[:, None] == target[None, :, k]).astype(BF16)
    high = combine.astype(BF16)
    low = (combine - high.astype(F32)).astype(BF16)

    outgoing = jnp.dot(choose, expert_in, preferred_element_type=F32).astype(BF16)
    got = lax.all_to_all(
        outgoing.reshape(experts, slots, model), ("sp", "dp"), split_axis=0, concat_axis=0, tiled=True
    )
    own = expert_gate.shape[0]
    shaped = got.reshape(ranks, own, slots, model)
    if own == 1:
        flat = got.reshape(ranks * slots, model)
        gate = jnp.dot(flat, expert_gate[0], preferred_element_type=F32)
        up = jnp.dot(flat, expert_up[0], preferred_element_type=F32)
        hidden = (jax.nn.silu(gate) * up).astype(BF16)
        done = jnp.dot(hidden, expert_down[0], preferred_element_type=F32).astype(BF16)
    else:
        gate = jnp.einsum("aenc,ecf->aenf", shaped, expert_gate, preferred_element_type=F32)
        up = jnp.einsum("aenc,ecf->aenf", shaped, expert_up, preferred_element_type=F32)
        hidden = (jax.nn.silu(gate) * up).astype(BF16)
        done = jnp.einsum("aenf,efc->aenc", hidden, expert_down, preferred_element_type=F32).astype(BF16)
    returned = lax.all_to_all(
        done.reshape(experts, slots, model), ("sp", "dp"), split_axis=0, concat_axis=0, tiled=True
    ).reshape(experts * slots, model)
    shared_hidden = (
        jax.nn.silu(jnp.dot(expert_in, shared_gate, preferred_element_type=F32))
        * jnp.dot(expert_in, shared_up, preferred_element_type=F32)
    ).astype(BF16)
    shared = mixed_f + jnp.dot(shared_hidden, shared_down, preferred_element_type=F32)
    routed = jnp.dot(high, returned, preferred_element_type=F32) + jnp.dot(
        low, returned, preferred_element_type=F32
    )
    return (shared + routed).astype(BF16)[None]


def solution(mesh):
    rows = P("dp", "sp", None)
    split = P(("sp", "dp"), None, None)
    return jax.shard_map(
        body,
        mesh=mesh,
        in_specs=(rows,) * 6 + (P(),) * 7 + (P("dp", None),) + (P(),) * 4 + (split,) * 3 + (rows,) * 2,
        out_specs=rows,
        check_vma=False,
    )
```

profile of v0, /device:TPU:17, one launch (start us, length us, event | category | flops | bytes accessed | tf_op | source)
XLA Modules:
  0.0 199.5 jit_solution(4572871299217062509)
XLA Ops:
  6.5 0.0 copy-start
  6.5 0.0 copy-start.11
  6.6 0.0 copy-start.12
  6.6 0.0 copy-start.8
  6.6 0.0 copy-start.9
  6.6 0.0 copy-start.10
  6.6 0.0 all-gather.2.cloned.1.call-start
  6.6 0.7 all-gather.2.cloned.1.call-update
  7.3 0.3 copy-done.6
  7.6 0.7 slice_bitcast_fusion.1
  8.4 0.0 copy-done.5
  8.4 3.1 %collective-permute-start = (bf16[8,4096]{1,0:T(8,128)(2,1)S(1)}, bf16[8,4096]{1,0:T(8,128)(2,1)S(1)}, u32[]{:S(2)}, u32[]{:S(2)}) collective-permute-start(bf16[8,4096]{1,0:T(8,128)(2,1)S(1)} %pad_maximum_fusion), channel_id=1, source_target_pairs={{0,4},{4,8},{8,12},{12,16},{16,20},{20,24},{24,28},{1,5},{5,9},{9,... | collective-permute-start | bytes 196616 | tf_op jit(solution)/shard_map/ppermute | solution.py:169
  11.5 0.0 copy-done.17
  11.5 0.1 copy.28
  11.7 0.0 copy-done.20
  11.7 0.1 broadcast_in_dim.48
  11.7 0.1 broadcast_in_dim_reshape.3.refs_10_
  11.8 2.5 %collective-permute-done.refs_3_ = bf16[8,4096]{1,0:T(8,128)(2,1)S(1)} collective-permute-done((bf16[8,4096]{1,0:T(8,128)(2,1)S(1)}, bf16[8,4096]{1,0:T(8,128)(2,1)S(1)}, u32[]{:S(2)}, u32[]{:S(2)}) %collective-permute-start) | collective-permute-done | bytes 65568 | tf_op jit(solution)/shard_map/ppermute | solution.py:169
  14.3 0.0 copy-done.11
  14.3 0.0 copy-done.12
  14.3 0.0 copy-done.8
  14.3 0.0 copy-done.9
  14.3 0.0 copy-done.10
  14.3 0.0 copy-start.7
  14.3 0.9 copy-done.7
  15.3 4.9 %shard_map.217 = (f32[128,2048]{1,0:T(8,128)S(1)}, bf16[128,1024]{1,0:T(8,128)(2,1)S(1)}, f32[128,32]{1,0:T(8,128)S(1)}, bf16[8,272,128]{2,1,0:T(8,128)(2,1)S(1)}) custom-call(bf16[128,2048]{1,0:T(8,128)(2,1)S(1)} %bitcast.59, bf16[128,1024]{1,0:T(8,128)(2,1)S(1)} %bitcast.60, bf16[128,1024]{1,0:T(8,128)(2,1)S(1)} %bitcast.61, ...), custom_call_target="tpu_custom_call" | custom-call | flops 400000000 | bytes 5000000 | tf_op jit(solution)/shard_map/pallas_call | solution.py:170
  20.1 0.0 copy-start.1
  20.2 1.0 copy-done.1
  21.2 18.4 %all_to_all.20.refs_0_ = bf16[8,272,128]{2,1,0:T(8,128)(2,1)S(1)} all-to-all(bf16[8,272,128]{2,1,0:T(8,128)(2,1)S(1)} %get-tuple-element.12), channel_id=1, replica_groups=mesh['sp'=8,'dp'=4] {'sp'}, dimensions={0} | all-to-all | bytes 1114112 | tf_op jit(solution)/shard_map/all_to_all | solution.py:186
  39.6 1.0 shard_map.218
  40.6 4.6 %all-to-all-start.1 = ((bf16[8,256,128]{2,1,0:T(8,128)(2,1)}), bf16[8,256,128]{2,1,0:T(8,128)(2,1)S(1)}, u32[]{:S(2)}, u32[]{:S(2)}) async-start(bf16[8,256,128]{2,1,0:T(8,128)(2,1)} %shard_map.218), calls=%async_computation.1 | async-start | bytes 1048576 | tf_op jit(solution)/shard_map/all_to_all | solution.py:195
  45.2 0.0 copy-done.18
  45.2 0.1 copy.29
  45.3 0.1 eq.71
  45.5 0.2 fusion.17
  45.7 0.1 convert_element_type.68
  45.9 0.2 slice_reduce_fusion.1
  46.0 10.7 %all-to-all-done.1 = bf16[8,256,128]{2,1,0:T(8,128)(2,1)S(1)} async-done(((bf16[8,256,128]{2,1,0:T(8,128)(2,1)}), bf16[8,256,128]{2,1,0:T(8,128)(2,1)S(1)}, u32[]{:S(2)}, u32[]{:S(2)}) %all-to-all-start.1) | async-done | bytes 524320 | tf_op jit(solution)/shard_map/all_to_all | solution.py:195
  56.7 0.0 copy-done.4
  56.7 1.2 copy-done.2
  58.0 1.0 copy-done.3
  59.0 1.5 shard_map.219
  60.5 0.0 copy-start.16
  60.5 8.2 %all-gather.2.cloned.1.call-done = bf16[2048,2048]{1,0:T(8,128)(2,1)} async-done(((bf16[512,2048]{1,0:T(8,128)(2,1)}), bf16[2048,2048]{1,0:T(8,128)(2,1)}) %all-gather.2.cloned.1.call-update) | async-done | bytes 8388624 | tf_op jit(solution)/shard_map/all_gather | solution.py:167
  68.7 4.8 %multiply_reduce_fusion = (f32[128]{0:T(128)S(1)}, f32[128,2048]{1,0:T(8,128)S(1)}) fusion(bf16[128,2048]{1,0:T(8,128)(2,1)S(1)} %shard_map.219, bf16[2048,2048]{1,0:T(8,128)(2,1)} %all-gather.2.cloned.1.call-done, bf16[1,128,2048]{2,1,0:T(8,128)(2,1)} %param.23), kind=kOutput, calls=%fused_computation.22 | convolution fusion | flops 1075314560 | bytes 10486272 | tf_op jit(solution)/shard_map/dot_general | solution.py:205
  73.6 0.0 copy-start.13
  73.6 0.0 copy-done.16
  73.6 0.8 convolution_convert_fusion
  74.4 0.0 copy-start.21
  74.4 52.1 %all_to_all.21 = bf16[32,16,2048]{2,1,0:T(8,128)(2,1)} all-to-all(bf16[32,16,2048]{2,1,0:T(8,128)(2,1)S(1)} %bitcast.64), channel_id=1, replica_groups=mesh['sp'=8,'dp'=4] {'sp','dp'}, dimensions={0} | all-to-all | bytes 4194304 | tf_op jit(solution)/shard_map/all_to_all | solution.py:232
  126.5 0.0 copy-done.13
  126.5 0.0 copy-done.21
  126.5 2.8 %fusion.8 = f32[512,512]{1,0:T(8,128)S(1)} fusion(bf16[512,2048]{1,0:T(8,128)(2,1)} %bitcast.18, bf16[1,2048,512]{2,1,0:T(8,128)(2,1)S(1)} %copy-done.21), kind=kOutput, calls=%fused_computation.13 | convolution fusion | flops 1073741824 | bytes 5242880 | tf_op jit(solution)/shard_map/dot_general | solution.py:239
  129.4 0.0 copy-done
  129.4 6.0 %convolution_convert_fusion.1 = bf16[512,2048]{1,0:T(8,128)(2,1)} fusion(bf16[1,512,2048]{2,1,0:T(8,128)(2,1)S(1)} %copy-done, bf16[512,2048]{1,0:T(8,128)(2,1)} %bitcast.18, bf16[1,2048,512]{2,1,0:T(8,128)(2,1)} %param.42, f32[512,512]{1,0:T(8,128)S(1)} %fusion.8), kind=kOutput, calls=%fused_computation.1 | convolution fusion | flops 2150105088 | bytes 9437184 | tf_op jit(solution)/shard_map/dot_general | solution.py:242
  135.4 4.9 %all-to-all-start.3 = ((bf16[32,16,2048]{2,1,0:T(8,128)(2,1)}), bf16[32,16,2048]{2,1,0:T(8,128)(2,1)}, u32[]{:S(2)}, u32[]{:S(2)}) async-start(bf16[32,16,2048]{2,1,0:T(8,128)(2,1)} %bitcast.65), calls=%async_computation.3 | async-start | bytes 4194304 | tf_op jit(solution)/shard_map/all_to_all | solution.py:248
  140.3 0.0 copy-done.19
  140.3 0.0 copy-done.14
  140.4 2.1 %fusion.49 = f32[128,512]{1,0:T(8,128)S(1)} fusion(bf16[2048,512]{1,0:T(8,128)(2,1)} %param.38, f32[128,2048]{1,0:T(8,128)S(1)} %copy-done.14, f32[2048]{0:T(1024)S(1)} %copy-done.16, f32[128]{0:T(128)S(1)} %add_rsqrt_fusion), kind=kOutput, calls=%fused_computation.66 | convolution fusion | flops 269221888 | bytes 3416576 | tf_op jit(solution)/shard_map/dot_general | solution.py:252
  142.4 4.1 %convolution_add_fusion.1 = f32[128,2048]{1,0:T(8,128)} fusion(f32[128,2048]{1,0:T(8,128)S(1)} %copy-done.14, bf16[512,2048]{1,0:T(8,128)(2,1)} %param.40, bf16[2048,512]{1,0:T(8,128)(2,1)} %param.39, f32[128,512]{1,0:T(8,128)S(1)} %fusion.49, f32[2048]{0:T(1024)S(1)} %copy-done.16, f32[128]{0:T(128)S(1)} %add_rsqrt_fusion), kind=kOutput, calls=%fused_computation.4 | convolution fusion | flops 538312704 | bytes 6562304 | tf_op jit(solution)/shard_map/dot_general | solution.py:255
  146.5 41.1 %all-to-all-done.3 = bf16[32,16,2048]{2,1,0:T(8,128)(2,1)} async-done(((bf16[32,16,2048]{2,1,0:T(8,128)(2,1)}), bf16[32,16,2048]{2,1,0:T(8,128)(2,1)}, u32[]{:S(2)}, u32[]{:S(2)}) %all-to-all-start.3) | async-done | bytes 2097184 | tf_op jit(solution)/shard_map/all_to_all | solution.py:248
  187.6 2.1 %fusion.41 = f32[128,2048]{1,0:T(8,128)S(1)} fusion(bf16[512,2048]{1,0:T(8,128)(2,1)} %bitcast.23, f32[128]{0:T(128)S(1)} %get-tuple-element.16, s32[128]{0:T(128)S(1)} %get-tuple-element.14, f32[128]{0:T(128)S(1)} %get-tuple-element.15, s32[128]{0:T(128)S(1)} %get-tuple-element.13), kind=kOutput, calls=%fused_computation.48 | convolution fusion | flops 268828672 | bytes 3147776 | tf_op jit(solution)/shard_map/dot_general | solution.py:256
  189.7 0.0 copy-done.15
  189.7 3.0 %fusion.4 = bf16[1,128,2048]{2,1,0:T(8,128)(2,1)} fusion(f32[128,2048]{1,0:T(8,128)S(1)} %copy-done.15, f32[128,2048]{1,0:T(8,128)S(1)} %fusion.41, bf16[512,2048]{1,0:T(8,128)(2,1)} %bitcast.23, f32[128]{0:T(128)S(1)} %get-tuple-element.16, s32[128]{0:T(128)S(1)} %get-tuple-element.14, f32[128]{0:T(128)S(1)} %get-tuple-element.15, s32[128]{0:T(128)S(1)} %get-tuple-element.13), kind=kOutput, calls=%fused_computation.9 | convolution fusion | flops 269811712 | bytes 4720640 | tf_op jit(solution)/shard_map/dot_general | solution.py:256
  (17 shorter events, 0.1 us)
Async XLA Ops:
  6.5 122.9 %copy-start = (bf16[1,512,2048]{2,1,0:T(8,128)(2,1)S(1)}, bf16[1,512,2048]{2,1,0:T(8,128)(2,1)}, u32[]{:S(2)}) copy-start(bf16[1,512,2048]{2,1,0:T(8,128)(2,1)} %param.43) | copy-start | bytes 6291460
  6.5 1.1 copy-start.6
  6.5 1.8 copy-start.5
  6.5 5.0 %copy-start.17 = (bf16[1,128,32]{1,2,0:T(8,128)(2,1)S(1)}, bf16[1,128,32]{1,2,0:T(8,128)(2,1)}, u32[]{:S(2)}) copy-start(bf16[1,128,32]{1,2,0:T(8,128)(2,1)} %param.28) | copy-start | bytes 24580
  6.5 5.1 %copy-start.20 = (f32[32]{0:T(128)S(1)}, f32[32]{0:T(128)}, u32[]{:S(2)}) copy-start(f32[32]{0:T(128)} %param.34) | copy-start | bytes 388
  6.5 7.7 %copy-start.11 = (f32[32]{0:T(128)S(1)}, f32[32]{0:T(128)}, u32[]{:S(2)}) copy-start(f32[32]{0:T(128)} %param.32) | copy-start | bytes 388
  6.6 7.7 %copy-start.12 = (f32[32]{0:T(128)S(1)}, f32[32]{0:T(128)}, u32[]{:S(2)}) copy-start(f32[32]{0:T(128)} %param.33) | copy-start | bytes 388
  6.6 7.7 %copy-start.8 = (bf16[4,2048]{1,0:T(4,128)(2,1)S(1)}, bf16[4,2048]{1,0:T(4,128)(2,1)}, u32[]{:S(2)}) copy-start(bf16[4,2048]{1,0:T(4,128)(2,1)} %refs_5_.1) | copy-start | bytes 49156
  6.6 7.7 %copy-start.9 = (bf16[4,1024]{1,0:T(4,128)(2,1)S(1)}, bf16[4,1024]{1,0:T(4,128)(2,1)}, u32[]{:S(2)}) copy-start(bf16[4,1024]{1,0:T(4,128)(2,1)} %refs_6_.1) | copy-start | bytes 24580
  6.6 7.7 %copy-start.10 = (bf16[4,1024]{1,0:T(4,128)(2,1)S(1)}, bf16[4,1024]{1,0:T(4,128)(2,1)}, u32[]{:S(2)}) copy-start(bf16[4,1024]{1,0:T(4,128)(2,1)} %refs_7_.1) | copy-start | bytes 24580
  6.6 62.1 %all-gather.2.cloned.1.call-start = ((), (), s32[]{:S(2)}) async-start(), calls=%async_computation.4 | async-start | bytes 10485760 | tf_op jit(solution)/shard_map/all_gather | solution.py:167
  8.4 5.9 %collective-permute-start = (bf16[8,4096]{1,0:T(8,128)(2,1)S(1)}, bf16[8,4096]{1,0:T(8,128)(2,1)S(1)}, u32[]{:S(2)}, u32[]{:S(2)}) collective-permute-start(bf16[8,4096]{1,0:T(8,128)(2,1)S(1)} %pad_maximum_fusion), channel_id=1, source_target_pairs={{0,4},{4,8},{8,12},{12,16},{16,20},{20,24},{24,28},{1,5},{5,9},{9,... | collective-permute-start | bytes 196616 | tf_op jit(solution)/shard_map/ppermute | solution.py:169
  14.3 1.0 copy-start.7
  20.1 1.1 copy-start.1
  21.2 24.0 %copy-start.18 = (s32[1,128,2]{1,2,0:T(2,128)S(1)}, s32[1,128,2]{1,2,0:T(2,128)}, u32[]{:S(2)}) copy-start(s32[1,128,2]{1,2,0:T(2,128)} %param.44) | copy-start | bytes 3076
  21.2 35.5 %copy-start.4 = (f32[2048]{0:T(1024)S(1)}, f32[2048]{0:T(1024)}, u32[]{:S(2)}) copy-start(f32[2048]{0:T(1024)} %param.35) | copy-start | bytes 24580
  40.6 16.1 %all-to-all-start.1 = ((bf16[8,256,128]{2,1,0:T(8,128)(2,1)}), bf16[8,256,128]{2,1,0:T(8,128)(2,1)S(1)}, u32[]{:S(2)}, u32[]{:S(2)}) async-start(bf16[8,256,128]{2,1,0:T(8,128)(2,1)} %shard_map.218), calls=%async_computation.1 | async-start | bytes 1048576 | tf_op jit(solution)/shard_map/all_to_all | solution.py:195
  56.7 1.2 copy-start.2
  58.0 1.0 copy-start.3
  60.5 13.1 %copy-start.16 = (f32[2048]{0:T(1024)S(1)}, f32[2048]{0:T(1024)}, u32[]{:S(2)}) copy-start(f32[2048]{0:T(1024)} %param.37) | copy-start | bytes 24580
  73.6 53.0 %copy-start.13 = (f32[128,2048]{1,0:T(8,128)}, f32[128,2048]{1,0:T(8,128)S(1)}, u32[]{:S(2)}) copy-start(f32[128,2048]{1,0:T(8,128)S(1)} %get-tuple-element.18) | copy-start | bytes 3145732
  74.4 52.2 %copy-start.21 = (bf16[1,2048,512]{2,1,0:T(8,128)(2,1)S(1)}, bf16[1,2048,512]{2,1,0:T(8,128)(2,1)}, u32[]{:S(2)}) copy-start(bf16[1,2048,512]{2,1,0:T(8,128)(2,1)} %param.41) | copy-start | bytes 6291460
  135.4 5.0 %copy-start.19 = (f32[1,128,2]{1,2,0:T(2,128)S(1)}, f32[1,128,2]{1,2,0:T(2,128)}, u32[]{:S(2)}) copy-start(f32[1,128,2]{1,2,0:T(2,128)} %param.45) | copy-start | bytes 3076
  135.4 5.0 %copy-start.14 = (f32[128,2048]{1,0:T(8,128)S(1)}, f32[128,2048]{1,0:T(8,128)}, u32[]{:S(2)}) copy-start(f32[128,2048]{1,0:T(8,128)} %copy-done.13) | copy-start | bytes 3145732
  135.4 52.2 %all-to-all-start.3 = ((bf16[32,16,2048]{2,1,0:T(8,128)(2,1)}), bf16[32,16,2048]{2,1,0:T(8,128)(2,1)}, u32[]{:S(2)}, u32[]{:S(2)}) async-start(bf16[32,16,2048]{2,1,0:T(8,128)(2,1)} %bitcast.65), calls=%async_computation.3 | async-start | bytes 4194304 | tf_op jit(solution)/shard_map/all_to_all | solution.py:248
  146.5 43.2 %copy-start.15 = (f32[128,2048]{1,0:T(8,128)S(1)}, f32[128,2048]{1,0:T(8,128)}, u32[]{:S(2)}) copy-start(f32[128,2048]{1,0:T(8,128)} %convolution_add_fusion.1) | copy-start | bytes 3145732
Sparse Core Ops, SparseCore 0:
  9.0 59.7 all-gather.1
where the time goes:
time: 203 us; the launch traced here: 200 us
  blocking collectives  70.5 us (35%)
  waiting for transfers between devices  63.2 us (31%)
  matrix products  25.9 us (13%)
  between operations  13.7 us (7%)
  starting transfers between devices  12.8 us (6%)
  Pallas kernels  7.34 us (4%)
  local copies, waits for them, and re-layouts  6.19 us (3%)
    all_to_all x1, blocking collectives, body(): lax.all_to_all(outgoing.reshape(experts, slots, model), ('sp', 'dp'), spl...  52.1 us
    all_to_all x1, waiting for transfers between devices, body(): lax.all_to_all(done.reshape(experts, slots, model), ('sp', 'dp'), split_a...  41.1 us
    all_to_all x1, blocking collectives, body(): lax.all_to_all(states, 'sp', split_axis=0, concat_axis=0, tiled=True)  18.4 us
    all_to_all x1, waiting for transfers between devices, body(): lax.all_to_all(prefix, 'sp', split_axis=0, concat_axis=0, tiled=True)  10.7 us
    all_gather x1, waiting for transfers between devices, body(): weight = lax.all_gather(out_weight, 'dp', axis=0, tiled=True)  8.23 us
    dot_general x1, matrix products, body(): jnp.dot(hidden, expert_down[0], preferred_element_type=F32).astype(BF16)  5.97 us
    all_to_all x1, starting transfers between devices, body(): lax.all_to_all(done.reshape(experts, slots, model), ('sp', 'dp'), split_a...  4.94 us
    unnamed x46, local copies, waits for them, and re-layouts  4.87 us
  transfers between devices with their start and end apart: 4, of which 4 were waited for; matrix products, arithmetic and copies ran while one was open for 4% of the time, Pallas kernels for 4%

commit v1 on v0

--- a/solution.py
+++ b/solution.py
@@ -11,6 +11,8 @@
 TAIL = 16
 F32 = jnp.float32
 BF16 = jnp.bfloat16
+MESH = pl.DeviceIdType.MESH
+CHUNKS = 4
 
 
 def silu(v):
@@ -142,6 +144,303 @@
         out_ref[:, xcol] = (v * gain_ref[:, xcol]).astype(BF16)
 
 
+def pick(index, table):
+    value = jnp.int32(table[0])
+    for c in range(1, len(table)):
+        value = jnp.where(index == c, jnp.int32(table[c]), value)
+    return value
+
+
+def layer_of_steps(depth):
+    if depth == 4:
+        mid, end = (1, 2), (0, 3)
+        return [
+            ("take", 1, None), ("take", 2, mid), ("give", 1, None), ("give", 2, mid), ("expert", 0, None),
+            ("expert", 1, None), ("join", 0, None), ("take", 2, end), ("give", 2, end), ("take", 3, mid),
+            ("give", 3, mid), ("join", 1, None), ("expert", 2, None), ("take", 3, end), ("give", 3, end),
+            ("join", 2, None), ("expert", 3, None), ("join", 3, None),
+        ]
+    steps = [("expert", 0, None), ("join", 0, None)]
+    for k in range(1, depth):
+        steps += [("take", k, None), ("give", k, None), ("expert", k, None), ("join", k, None)]
+    return steps
+
+
+def moe_kernel(*refs, depth, side, ndp, picks, blocks):
+    normed_ref, resid_ref, gain_ref, info_ref = refs[:4]
+    w_ref = refs[4]
+    shared_refs = refs[5:8]
+    expert_refs = refs[8:11]
+    out_ref = refs[11]
+    (
+        w_buf, sg_buf, su_buf, sd_buf, eg_buf, eu_buf, ed_buf, t_buf, info_buf, g_buf, x_buf, r_buf, p_buf, q_buf,
+        acc, local_sem, info_send, info_recv, t_send, t_recv, g_send, x_recv, d_send, r_recv, c_send, q_recv,
+    ) = refs[12:]
+    tokens, model = t_buf.shape[1:]
+    plane, slots = g_buf.shape[1:3]
+    lanes = plane * slots
+    rows = tokens // CHUNKS
+    tile = min(512, model)
+    sp, dp = lax.axis_index("sp"), lax.axis_index("dp")
+    zi, me = sp // side, (sp % side) * ndp + dp
+    order = [[z] + sorted((s for s in range(depth) if s != z), key=lambda s: (abs(s - z), s)) for z in range(depth)]
+    source = [pick(zi, [order[z][k] for z in range(depth)]) for k in range(depth)]
+
+    def peer(q):
+        return (zi * side + q // ndp, q % ndp)
+
+    def along(step):
+        return (sp + step * side, dp)
+
+    barrier = pltpu.get_barrier_semaphore()
+
+    @pl.loop(1, plane)
+    def _(j):
+        pl.semaphore_signal(barrier, inc=1, device_id=peer((me + j) % plane), device_id_type=MESH)
+
+    @pl.loop(1, depth)
+    def _(j):
+        pl.semaphore_signal(
+            barrier, inc=1, device_id=((zi + j) % depth * side + sp % side, dp), device_id_type=MESH
+        )
+
+    w_rows = w_buf.shape[1]
+    loads = []
+    for i in range(blocks):
+        loads.append(pltpu.make_async_copy(w_ref.at[pl.ds(i * w_rows, w_rows)], w_buf.at[i], local_sem.at[i]))
+    for i, (a, b) in enumerate(zip(shared_refs, (sg_buf, su_buf, sd_buf))):
+        loads.append(pltpu.make_async_copy(a, b, local_sem.at[blocks + i]))
+    for i, (a, b) in enumerate(zip(expert_refs, (eg_buf, eu_buf, ed_buf))):
+        loads.append(pltpu.make_async_copy(a.at[0], b, local_sem.at[blocks + 3 + i]))
+    for c in loads:
+        c.start()
+
+    for i in range(blocks):
+        loads[i].wait()
+    square = jnp.zeros((tokens, 1), F32)
+    for n in range(0, model, tile):
+        cols = slice(n, n + tile)
+        total = resid_ref[:, cols].astype(F32)
+        for i in range(blocks):
+            total = total + jnp.dot(
+                normed_ref[:, i * w_rows : (i + 1) * w_rows], w_buf[i, :, cols], preferred_element_type=F32
+            )
+        total = total.astype(BF16).astype(F32)
+        acc[:, cols] = total
+        square = square + jnp.sum(total * total, axis=1, keepdims=True)
+    scale = lax.rsqrt(square / model + EPS)
+    for n in range(0, model, tile):
+        cols = slice(n, n + tile)
+        t_buf[zi, :, cols] = (acc[:, cols] * scale * gain_ref[:, cols]).astype(BF16)
+    info_buf[zi] = info_ref[...]
+
+    pl.semaphore_wait(barrier, plane - 1 + depth - 1)
+
+    @pl.loop(1, depth)
+    def _(j):
+        pltpu.make_async_remote_copy(
+            src_ref=info_ref, dst_ref=info_buf.at[zi], send_sem=info_send, recv_sem=info_recv.at[zi],
+            device_id=((zi + j) % depth * side + sp % side, dp), device_id_type=MESH,
+        ).start()
+
+    def token_copy(s, j, up):
+        part = pl.ds(j * rows, rows)
+        return pltpu.make_async_remote_copy(
+            src_ref=t_buf.at[s, part], dst_ref=t_buf.at[s, part], send_sem=t_send.at[1 if up else 0, s],
+            recv_sem=t_recv.at[s, j], device_id=along(1 if up else -1), device_id_type=MESH,
+        )
+
+    def sum_copy(s, j, up):
+        part = pl.ds(j * rows, rows)
+        into = s if up else jnp.where(s == zi - 1, depth, s)
+        return pltpu.make_async_remote_copy(
+            src_ref=p_buf.at[s, part], dst_ref=q_buf.at[into, part], send_sem=c_send.at[s],
+            recv_sem=q_recv.at[into, j], device_id=along(1 if up else -1), device_id_type=MESH,
+        )
+
+    def send_sum(s, j):
+        @pl.when(s > zi)
+        def _():
+            sum_copy(s, j, True).start()
+
+        @pl.when(s < zi)
+        def _():
+            sum_copy(s, j, False).start()
+
+    def send_tokens(s, j):
+        @pl.when((s <= zi) & (zi < depth - 1))
+        def _():
+            token_copy(s, j, True).start()
+
+        @pl.when((s >= zi) & (zi > 0))
+        def _():
+            token_copy(s, j, False).start()
+
+    def landed(ref, sem):
+        pltpu.make_async_copy(ref, ref, sem).wait()
+
+    def take(k):
+        s = source[k]
+        landed(info_buf.at[s], info_recv.at[s])
+        for j in range(CHUNKS):
+            landed(t_buf.at[s, pl.ds(j * rows, rows)], t_recv.at[s, j])
+            send_tokens(s, j)
+
+    def target():
+        row = lax.broadcasted_iota(jnp.int32, (lanes, tokens), 0) + zi * lanes
+        return row.astype(F32)
+
+    def give(k):
+        s = source[k]
+        info = info_buf[s]
+        slot = target()
+        chosen = slot == info[0:1]
+        for p in range(1, picks):
+            chosen = chosen | (slot == info[p : p + 1])
+        chosen = jnp.where(chosen, 1.0, 0.0).astype(BF16)
+        for n in range(0, model, tile):
+            cols = slice(n, n + tile)
+            part = jnp.dot(chosen, t_buf[s, :, cols], preferred_element_type=F32).astype(BF16)
+            g_buf[s, :, :, cols] = part.reshape(plane, slots, tile)
+
+        @pl.loop(1, plane)
+        def _(j):
+            q = (me + j) % plane
+            pltpu.make_async_remote_copy(
+                src_ref=g_buf.at[s, q], dst_ref=x_buf.at[s, me], send_sem=g_send.at[s], recv_sem=x_recv.at[s],
+                device_id=peer(q), device_id_type=MESH,
+            ).start()
+
+        x_buf[s, me] = g_buf[s, me]
+
+    def expert(k):
+        s = source[k]
+        if k == 0:
+            for c in loads[blocks + 3 :]:
+                c.wait()
+        landed(x_buf.at[s, pl.ds(0, plane - 1)], x_recv.at[s])
+        rows_in = x_buf[s].reshape(lanes, model)
+        gate = jnp.dot(rows_in, eg_buf[...], preferred_element_type=F32)
+        up = jnp.dot(rows_in, eu_buf[...], preferred_element_type=F32)
+        hidden = (silu(gate) * up).astype(BF16)
+        for n in range(0, model, tile):
+            cols = slice(n, n + tile)
+            part = jnp.dot(hidden, ed_buf[:, cols], preferred_element_type=F32).astype(BF16)
+            x_buf[s, :, :, cols] = part.reshape(plane, slots, tile)
+
+        @pl.loop(1, plane)
+        def _(j):
+            q = (me + j) % plane
+            pltpu.make_async_remote_copy(
+                src_ref=x_buf.at[s, q], dst_ref=r_buf.at[s, me], send_sem=d_send.at[s], recv_sem=r_recv.at[s],
+                device_id=peer(q), device_id_type=MESH,
+            ).start()
+
+        r_buf[s, me] = x_buf[s, me]
+
+    def join(k):
+        s = source[k]
+        landed(r_buf.at[s, pl.ds(0, plane - 1)], r_recv.at[s])
+        info = info_buf[s]
+        slot = target()
+        weight = jnp.zeros((lanes, tokens), F32)
+        for p in range(picks):
+            weight = weight + jnp.where(slot == info[p : p + 1], info[picks + p : picks + p + 1], 0.0)
+        high = weight.astype(BF16)
+        low = (weight - high.astype(F32)).astype(BF16)
+        for n in range(0, model, tile):
+            cols = slice(n, n + tile)
+            block = r_buf[s, :, :, cols].reshape(lanes, tile)
+            part = lax.dot_general(high, block, (((0,), (0,)), ((), ())), preferred_element_type=F32)
+            part = part + lax.dot_general(low, block, (((0,), (0,)), ((), ())), preferred_element_type=F32)
+            if k == 0:
+                acc[:, cols] = acc[:, cols] + part
+            else:
+                p_buf[s, :, cols] = part.astype(BF16)
+        if k:
+            @pl.when((zi == 0) | (zi == depth - 1))
+            def _():
+                for j in range(CHUNKS):
+                    send_sum(s, j)
+
+    for j in range(CHUNKS):
+        send_tokens(source[0], j)
+    give(0)
+
+    for c in loads[blocks : blocks + 3]:
+        c.wait()
+    x = t_buf[zi]
+    hidden = silu(jnp.dot(x, sg_buf[...], preferred_element_type=F32)) * jnp.dot(
+        x, su_buf[...], preferred_element_type=F32
+    )
+    hidden = hidden.astype(BF16)
+    for n in range(0, model, tile):
+        cols = slice(n, n + tile)
+        acc[:, cols] = acc[:, cols] + jnp.dot(hidden, sd_buf[:, cols], preferred_element_type=F32)
+
+    actions = {"take": take, "give": give, "expert": expert, "join": join}
+    for name, k, planes in layer_of_steps(depth):
+        if planes is None:
+            actions[name](k)
+        else:
+            taken = zi == planes[0]
+            for z in planes[1:]:
+                taken = taken | (zi == z)
+
+            @pl.when(taken)
+            def _(name=name, k=k):
+                actions[name](k)
+
+    def far(z, s):
+        return depth - 1 - s + depth - 1 - z if s < z else s + z
+
+    passing = [sorted((s for s in range(depth) if s != z), key=lambda s, z=z: (far(z, s), s)) for z in range(depth)]
+
+    @pl.when((zi > 0) & (zi < depth - 1))
+    def _():
+        for i in range(depth - 1):
+            s = pick(zi, [passing[z][i] for z in range(depth)])
+            for j in range(CHUNKS):
+                part = pl.ds(j * rows, rows)
+                landed(q_buf.at[s, part], q_recv.at[s, j])
+                p_buf[s, part] = (p_buf[s, part].astype(F32) + q_buf[s, part].astype(F32)).astype(BF16)
+                send_sum(s, j)
+
+    for j in range(CHUNKS):
+        part = pl.ds(j * rows, rows)
+
+        @pl.when(zi > 0)
+        def _():
+            landed(q_buf.at[zi, part], q_recv.at[zi, j])
+            acc[part] = acc[part] + q_buf[zi, part].astype(F32)
+
+        @pl.when(zi < depth - 1)
+        def _():
+            landed(q_buf.at[depth, part], q_recv.at[depth, j])
+            acc[part] = acc[part] + q_buf[depth, part].astype(F32)
+
+        out_ref[part] = acc[part].astype(BF16)
+
+    @pl.loop(1, depth)
+    def _(j):
+        landed(info_ref, info_send)
+
+    for k in range(depth):
+        s = source[k]
+        landed(g_buf.at[s, pl.ds(0, plane - 1)], g_send.at[s])
+        landed(x_buf.at[s, pl.ds(0, plane - 1)], d_send.at[s])
+        if k:
+            landed(p_buf.at[s], c_send.at[s])
+
+        @pl.when((s <= zi) & (zi < depth - 1))
+        def _():
+            landed(t_buf.at[s], t_send.at[1, s])
+
+        @pl.when((s >= zi) & (zi > 0))
+        def _():
+            landed(t_buf.at[s], t_send.at[0, s])
+
+
 def vmem(count):
     return [pl.BlockSpec(memory_space=pltpu.VMEM)] * count
 
@@ -164,6 +463,7 @@
     ways = lax.axis_size("sp")
     local = heads // ways
     x_rows, b_rows, c_rows = head_input[0], b_input[0], c_input[0]
+    ndp = lax.axis_size("dp")
     weight = lax.all_gather(out_weight, "dp", axis=0, tiled=True)
     tail = jnp.concatenate([x_rows[-HALO:], b_rows[-HALO:], c_rows[-HALO:]], axis=1)
     halo = lax.ppermute(tail, "sp", [(i, i + 1) for i in range(ways - 1)])
@@ -202,61 +502,59 @@
         cost_estimate=pl.CostEstimate(flops=100_000_000, bytes_accessed=3_000_000, transcendentals=400_000),
     )(y, cm, cum, before, gate_input[0], norm_gain[None])
 
-    mixed = (residual[0].astype(F32) + jnp.dot(normed, weight, preferred_element_type=F32)).astype(BF16)
-    mixed_f = mixed.astype(F32)
-    expert_in = (
-        mixed_f * lax.rsqrt(jnp.mean(mixed_f * mixed_f, axis=1, keepdims=True) + EPS) * ffn_gain[None, :]
-    ).astype(BF16)
-
     picks = routes.shape[2]
-    ranks = ways * lax.axis_size("dp")
-    experts = ranks * expert_gate.shape[0]
-    slots = 2 * tokens * picks // experts
+    side = max(1, ndp // 2)
+    depth = ways // side
+    plane = side * ndp
+    experts = ways * ndp
+    slots = max(16, 2 * tokens * picks // experts)
     chosen = routes[0].reshape(-1)
     pairs = chosen.shape[0]
     onehot = (chosen[:, None] == jnp.arange(experts, dtype=jnp.int32)[None, :]).astype(BF16)
     earlier = (jnp.arange(pairs)[:, None] > jnp.arange(pairs)[None, :]).astype(BF16)
     counts = jnp.dot(earlier, onehot, preferred_element_type=F32)
-    position = jnp.sum(counts * onehot.astype(F32), axis=1).astype(jnp.int32)
-    target = (chosen * slots + position).reshape(tokens, picks)
-    lanes = jnp.arange(experts * slots, dtype=jnp.int32)
-    combine = jnp.zeros((tokens, experts * slots), F32)
-    choose = jnp.zeros((experts * slots, tokens), BF16)
-    for k in range(picks):
-        combine = combine + jnp.where(target[:, k, None] == lanes[None, :], route_weights[0][:, k, None], 0.0)
-        choose = choose + (lanes[:, None] == target[None, :, k]).astype(BF16)
-    high = combine.astype(BF16)
-    low = (combine - high.astype(F32)).astype(BF16)
-
-    outgoing = jnp.dot(choose, expert_in, preferred_element_type=F32).astype(BF16)
-    got = lax.all_to_all(
-        outgoing.reshape(experts, slots, model), ("sp", "dp"), split_axis=0, concat_axis=0, tiled=True
+    position = jnp.sum(counts * onehot.astype(F32), axis=1)
+    place = (chosen.astype(F32) * slots + position).reshape(tokens, picks)
+    info = jnp.concatenate([place.T, route_weights[0].T, jnp.zeros((8 - 2 * picks, tokens), F32)], axis=0)
+
+    hbm = [pl.BlockSpec(memory_space=pl.ANY)]
+    dma = pltpu.SemaphoreType.DMA
+    hidden = expert_gate.shape[2]
+    shared = shared_gate.shape[1]
+    out = pl.pallas_call(
+        lambda *refs: moe_kernel(*refs, depth=depth, side=side, ndp=ndp, picks=picks, blocks=ndp),
+        out_shape=jax.ShapeDtypeStruct((tokens, model), BF16),
+        in_specs=vmem(4) + hbm * 7,
+        out_specs=vmem(1)[0],
+        scratch_shapes=[
+            pltpu.VMEM((ndp, inner // ndp, model), BF16),
+            pltpu.VMEM((model, shared), BF16),
+            pltpu.VMEM((model, shared), BF16),
+            pltpu.VMEM((shared, model), BF16),
+            pltpu.VMEM((model, hidden), BF16),
+            pltpu.VMEM((model, hidden), BF16),
+            pltpu.VMEM((hidden, model), BF16),
+            pltpu.VMEM((depth, tokens, model), BF16),
+            pltpu.VMEM((depth, 8, tokens), F32),
+            pltpu.VMEM((depth, plane, slots, model), BF16),
+            pltpu.VMEM((depth, plane, slots, model), BF16),
+            pltpu.VMEM((depth, plane, slots, model), BF16),
+            pltpu.VMEM((depth, tokens, model), BF16),
+            pltpu.VMEM((depth + 1, tokens, model), BF16),
+            pltpu.VMEM((tokens, model), F32),
+            dma((ndp + 6,)),
+            dma, dma((depth,)), dma((2, depth)), dma((depth, CHUNKS)), dma((depth,)), dma((depth,)),
+            dma((depth,)), dma((depth,)), dma((depth,)), dma((depth + 1, CHUNKS)),
+        ],
+        compiler_params=pltpu.CompilerParams(
+            vmem_limit_bytes=61 * 1024 * 1024, collective_id=1, has_side_effects=True
+        ),
+        cost_estimate=pl.CostEstimate(flops=8_000_000_000, bytes_accessed=24_000_000, transcendentals=500_000),
+    )(
+        normed, residual[0], ffn_gain[None], info, weight, shared_gate, shared_up, shared_down,
+        expert_gate, expert_up, expert_down,
     )
-    own = expert_gate.shape[0]
-    shaped = got.reshape(ranks, own, slots, model)
-    if own == 1:
-        flat = got.reshape(ranks * slots, model)
-        gate = jnp.dot(flat, expert_gate[0], preferred_element_type=F32)
-        up = jnp.dot(flat, expert_up[0], preferred_element_type=F32)
-        hidden = (jax.nn.silu(gate) * up).astype(BF16)
-        done = jnp.dot(hidden, expert_down[0], preferred_element_type=F32).astype(BF16)
-    else:
-        gate = jnp.einsum("aenc,ecf->aenf", shaped, expert_gate, preferred_element_type=F32)
-        up = jnp.einsum("aenc,ecf->aenf", shaped, expert_up, preferred_element_type=F32)
-        hidden = (jax.nn.silu(gate) * up).astype(BF16)
-        done = jnp.einsum("aenf,efc->aenc", hidden, expert_down, preferred_element_type=F32).astype(BF16)
-    returned = lax.all_to_all(
-        done.reshape(experts, slots, model), ("sp", "dp"), split_axis=0, concat_axis=0, tiled=True
-    ).reshape(experts * slots, model)
-    shared_hidden = (
-        jax.nn.silu(jnp.dot(expert_in, shared_gate, preferred_element_type=F32))
-        * jnp.dot(expert_in, shared_up, preferred_element_type=F32)
-    ).astype(BF16)
-    shared = mixed_f + jnp.dot(shared_hidden, shared_down, preferred_element_type=F32)
-    routed = jnp.dot(high, returned, preferred_element_type=F32) + jnp.dot(
-        low, returned, preferred_element_type=F32
-    )
-    return (shared + routed).astype(BF16)[None]
+    return out[None]
 
 
 def solution(mesh):

time: 203 us -> 177 us (0.87)
  the two profiles are of different devices: /device:TPU:17 before, /device:TPU:0 now
where the time goes in v1:
time: 177 us
  Pallas kernels  105 us (59%)
  waiting for transfers between devices  23.1 us (13%)
  blocking collectives  21.4 us (12%)
  between operations  13.6 us (8%)
  starting transfers between devices  8.43 us (5%)
  local copies, waits for them, and re-layouts  3.95 us (2%)
    pallas_call x1, Pallas kernels, body(): pl.pallas_call(lambda *refs: moe_kernel(*refs, depth=depth, side=side, nd...  97.8 us
    all_to_all x1, blocking collectives, body(): lax.all_to_all(states, 'sp', split_axis=0, concat_axis=0, tiled=True)  21.4 us
    all_to_all x1, waiting for transfers between devices, body(): lax.all_to_all(prefix, 'sp', split_axis=0, concat_axis=0, tiled=True)  12 us
    all_gather x1, waiting for transfers between devices, body(): weight = lax.all_gather(out_weight, 'dp', axis=0, tiled=True)  8.86 us
    ppermute x1, starting transfers between devices, body(): halo = lax.ppermute(tail, 'sp', [(i, i + 1) for i in range(ways - 1)])  4.9 us
    pallas_call x1, Pallas kernels, body(): pl.pallas_call(lambda *refs: block_kernel(*refs, groups=groups, local=loc...  4.86 us
  transfers between devices with their start and end apart: 3, of which 3 were waited for; matrix products, arithmetic and copies ran while one was open for 1% of the time, Pallas kernels for 4%

profile of v1, /device:TPU:0, one launch (start us, length us, event | category | flops | bytes accessed | tf_op | source)
XLA Modules:
  0.0 176.6 jit_solution(2811204769024392353)
XLA Ops:
  6.5 0.0 copy-start.4
  6.5 0.0 copy-start.5
  6.5 0.0 copy-start.3
  6.5 0.0 copy-start.11
  6.5 0.0 copy-start.14
  6.5 0.0 copy-start.9
  6.6 0.0 copy-start.10
  6.6 0.0 copy-start.6
  6.6 0.0 copy-start.7
  6.6 0.0 copy-start.8
  6.6 0.0 all-gather.2.cloned.1.call-start
  6.6 0.7 all-gather.2.cloned.1.call-update
  7.3 0.2 copy-done.4
  7.5 0.1 copy-done.5
  7.6 0.2 copy-done.3
  7.8 4.9 %collective-permute-start = (bf16[8,4096]{1,0:T(8,128)(2,1)S(1)}, bf16[8,4096]{1,0:T(8,128)(2,1)S(1)}, u32[]{:S(2)}, u32[]{:S(2)}) collective-permute-start(bf16[8,4096]{1,0:T(8,128)(2,1)S(1)} %pad_maximum_fusion), channel_id=1, source_target_pairs={{0,4},{4,8},{8,12},{12,16},{16,20},{20,24},{24,28},{1,5},{5,9},{9,... | collective-permute-start | bytes 196616 | tf_op jit(solution)/shard_map/ppermute | solution.py:469
  12.7 0.0 copy-done.11
  12.7 0.1 copy.25
  12.8 0.0 copy-done.14
  12.8 0.1 broadcast_in_dim.26
  12.9 0.1 broadcast_in_dim_reshape.3.refs_10_
  13.0 1.6 collective-permute-done.refs_3_
  14.5 0.0 copy-done.9
  14.5 0.0 copy-done.10
  14.6 0.0 copy-done.6
  14.6 0.0 copy-done.7
  14.6 0.0 copy-done.8
  14.6 4.9 %shard_map.217 = (f32[128,2048]{1,0:T(8,128)S(1)}, bf16[128,1024]{1,0:T(8,128)(2,1)S(1)}, f32[128,32]{1,0:T(8,128)S(1)}, bf16[8,272,128]{2,1,0:T(8,128)(2,1)S(1)}) custom-call(bf16[128,2048]{1,0:T(8,128)(2,1)S(1)} %bitcast.31, bf16[128,1024]{1,0:T(8,128)(2,1)S(1)} %bitcast.32, bf16[128,1024]{1,0:T(8,128)(2,1)S(1)} %bitcast.33, ...), custom_call_target="tpu_custom_call" | custom-call | flops 400000000 | bytes 5000000 | tf_op jit(solution)/shard_map/pallas_call | solution.py:470
  19.4 0.0 copy-start.12
  19.5 0.0 copy-start.13
  19.5 0.0 copy-start
  19.5 0.0 copy-start.2
  19.5 21.4 %all_to_all.10.refs_0_ = bf16[8,272,128]{2,1,0:T(8,128)(2,1)S(1)} all-to-all(bf16[8,272,128]{2,1,0:T(8,128)(2,1)S(1)} %get-tuple-element.12), channel_id=1, replica_groups=mesh['sp'=8,'dp'=4] {'sp'}, dimensions={0} | all-to-all | bytes 1114112 | tf_op jit(solution)/shard_map/all_to_all | solution.py:486
  40.9 1.0 shard_map.218
  41.9 3.5 %all-to-all-start.1 = ((bf16[8,256,128]{2,1,0:T(8,128)(2,1)}), bf16[8,256,128]{2,1,0:T(8,128)(2,1)S(1)}, u32[]{:S(2)}, u32[]{:S(2)}) async-start(bf16[8,256,128]{2,1,0:T(8,128)(2,1)} %shard_map.218), calls=%async_computation.1 | async-start | bytes 1048576 | tf_op jit(solution)/shard_map/all_to_all | solution.py:495
  45.4 0.0 copy-done.12
  45.4 0.1 copy.26
  45.5 0.1 eq.15
  45.7 0.2 fusion
  45.9 0.1 reduce_sum.12
  46.0 0.1 copy.27
  46.1 0.1 pad.2.clone
  46.2 0.0 copy-done.13
  46.2 0.7 maximum_maximum_fusion.refs_3_
  46.9 12.0 %all-to-all-done.1 = bf16[8,256,128]{2,1,0:T(8,128)(2,1)S(1)} async-done(((bf16[8,256,128]{2,1,0:T(8,128)(2,1)}), bf16[8,256,128]{2,1,0:T(8,128)(2,1)S(1)}, u32[]{:S(2)}, u32[]{:S(2)}) %all-to-all-start.1) | async-done | bytes 524320 | tf_op jit(solution)/shard_map/all_to_all | solution.py:495
  58.8 0.0 copy-done
  58.8 0.0 copy-done.2
  58.8 1.5 shard_map.219.refs_0_
  60.3 0.0 copy-start.1
  60.3 0.8 copy-done.1
  61.1 8.9 %all-gather.2.cloned.1.call-done.refs_4_ = bf16[2048,2048]{1,0:T(8,128)(2,1)} async-done(((bf16[512,2048]{1,0:T(8,128)(2,1)}), bf16[2048,2048]{1,0:T(8,128)(2,1)}) %all-gather.2.cloned.1.call-update) | async-done | bytes 8388624 | tf_op jit(solution)/shard_map/all_gather | solution.py:467
  70.0 97.8 %shard_map.220 = bf16[128,2048]{1,0:T(8,128)(2,1)} custom-call(bf16[128,2048]{1,0:T(8,128)(2,1)} %copy-done.1, bf16[128,2048]{1,0:T(8,128)(2,1)} %bitcast.38, f32[1,2048]{1,0:T(1,128)} %bitcast.39, f32[8,128]{1,0:T(8,128)} %maximum_maximum_fusion.refs_3_, bf16[2048,2048]{1,0:T(8,128)(2,1)} %all-gather.2.cloned.1.call-done.refs_4_, ...), custom_call_target="tpu_custom_call" | custom-call | flops 8000000000 | bytes 24000000 | tf_op jit(solution)/shard_map/pallas_call | solution.py:524
  167.8 1.9 %copy.29 = bf16[1,128,2048]{2,1,0:T(8,128)(2,1)} copy(bf16[1,128,2048]{2,1,0:T(8,128)(2,1)} %bitcast.36) | data formatting | bytes 1048576
  (5 shorter events, 0.0 us)
Async XLA Ops:
  6.5 0.9 copy-start.4
  6.5 1.0 copy-start.5
  6.5 1.2 copy-start.3
  6.5 6.1 %copy-start.11 = (bf16[1,128,32]{1,2,0:T(8,128)(2,1)S(1)}, bf16[1,128,32]{1,2,0:T(8,128)(2,1)}, u32[]{:S(2)}) copy-start(bf16[1,128,32]{1,2,0:T(8,128)(2,1)} %param.28) | copy-start | bytes 24580
  6.5 6.2 %copy-start.14 = (f32[32]{0:T(128)S(1)}, f32[32]{0:T(128)}, u32[]{:S(2)}) copy-start(f32[32]{0:T(128)} %param.34) | copy-start | bytes 388
  6.5 8.0 %copy-start.9 = (f32[32]{0:T(128)S(1)}, f32[32]{0:T(128)}, u32[]{:S(2)}) copy-start(f32[32]{0:T(128)} %param.32) | copy-start | bytes 388
  6.6 8.0 %copy-start.10 = (f32[32]{0:T(128)S(1)}, f32[32]{0:T(128)}, u32[]{:S(2)}) copy-start(f32[32]{0:T(128)} %param.33) | copy-start | bytes 388
  6.6 8.0 %copy-start.6 = (bf16[4,2048]{1,0:T(4,128)(2,1)S(1)}, bf16[4,2048]{1,0:T(4,128)(2,1)}, u32[]{:S(2)}) copy-start(bf16[4,2048]{1,0:T(4,128)(2,1)} %refs_5_.2) | copy-start | bytes 49156
  6.6 8.0 %copy-start.7 = (bf16[4,1024]{1,0:T(4,128)(2,1)S(1)}, bf16[4,1024]{1,0:T(4,128)(2,1)}, u32[]{:S(2)}) copy-start(bf16[4,1024]{1,0:T(4,128)(2,1)} %refs_6_.2) | copy-start | bytes 24580
  6.6 8.0 %copy-start.8 = (bf16[4,1024]{1,0:T(4,128)(2,1)S(1)}, bf16[4,1024]{1,0:T(4,128)(2,1)}, u32[]{:S(2)}) copy-start(bf16[4,1024]{1,0:T(4,128)(2,1)} %refs_7_.2) | copy-start | bytes 24580
  6.6 63.4 %all-gather.2.cloned.1.call-start = ((), (), s32[]{:S(2)}) async-start(), calls=%async_computation.2 | async-start | bytes 10485760 | tf_op jit(solution)/shard_map/all_gather | solution.py:467
  7.8 6.8 %collective-permute-start = (bf16[8,4096]{1,0:T(8,128)(2,1)S(1)}, bf16[8,4096]{1,0:T(8,128)(2,1)S(1)}, u32[]{:S(2)}, u32[]{:S(2)}) collective-permute-start(bf16[8,4096]{1,0:T(8,128)(2,1)S(1)} %pad_maximum_fusion), channel_id=1, source_target_pairs={{0,4},{4,8},{8,12},{12,16},{16,20},{20,24},{24,28},{1,5},{5,9},{9,... | collective-permute-start | bytes 196616 | tf_op jit(solution)/shard_map/ppermute | solution.py:469
  19.4 26.0 %copy-start.12 = (s32[1,128,2]{1,2,0:T(2,128)S(1)}, s32[1,128,2]{1,2,0:T(2,128)}, u32[]{:S(2)}) copy-start(s32[1,128,2]{1,2,0:T(2,128)} %param.44) | copy-start | bytes 3076
  19.5 26.7 %copy-start.13 = (f32[1,128,2]{1,2,0:T(2,128)S(1)}, f32[1,128,2]{1,2,0:T(2,128)}, u32[]{:S(2)}) copy-start(f32[1,128,2]{1,2,0:T(2,128)} %param.45) | copy-start | bytes 3076
  19.5 39.4 %copy-start = (bf16[1,128,2048]{2,1,0:T(8,128)(2,1)S(1)}, bf16[1,128,2048]{2,1,0:T(8,128)(2,1)}, u32[]{:S(2)}) copy-start(bf16[1,128,2048]{2,1,0:T(8,128)(2,1)} %param.25) | copy-start | bytes 1572868
  19.5 39.4 %copy-start.2 = (f32[2048]{0:T(1024)S(1)}, f32[2048]{0:T(1024)}, u32[]{:S(2)}) copy-start(f32[2048]{0:T(1024)} %param.35) | copy-start | bytes 24580
  41.9 16.9 %all-to-all-start.1 = ((bf16[8,256,128]{2,1,0:T(8,128)(2,1)}), bf16[8,256,128]{2,1,0:T(8,128)(2,1)S(1)}, u32[]{:S(2)}, u32[]{:S(2)}) async-start(bf16[8,256,128]{2,1,0:T(8,128)(2,1)} %shard_map.218), calls=%async_computation.1 | async-start | bytes 1048576 | tf_op jit(solution)/shard_map/all_to_all | solution.py:495
  60.3 0.8 copy-start.1
Sparse Core Ops, SparseCore 0:
  9.0 60.9 all-gather.1

commit v2 on v1

v2 whole, which is shorter than its diff:
```python
import jax
import jax.numpy as jnp
from jax import lax
from jax.experimental import pallas as pl
from jax.experimental.pallas import tpu as pltpu
from jax.sharding import PartitionSpec as P

EPS = 1e-06
HIGH = lax.Precision.HIGHEST
HALO = 8
TAIL = 16
PACK = 128
F32 = jnp.float32
BF16 = jnp.bfloat16
MESH = pl.DeviceIdType.MESH
CHUNKS = 4
PARTS = 4


def silu(v):
    return v * (1.0 / (1.0 + jnp.exp(-v)))


def conv_silu(halo, rows, taps):
    count = taps.shape[0]
    length = rows.shape[0]
    padded = jnp.concatenate([halo.astype(F32)[-HALO:], rows.astype(F32)], axis=0)
    total = None
    for tap in range(count):
        start = HALO - (count - 1) + tap
        term = padded[start : start + length] * taps[tap : tap + 1].astype(F32)
        total = term if total is None else total + term
    return silu(total)


def spread(columns, first, count, width):
    rows = columns.shape[0]
    return jnp.concatenate(
        [jnp.broadcast_to(columns[:, first + j : first + j + 1], (rows, width)) for j in range(count)],
        axis=1,
    )


def pick(index, table):
    value = jnp.int32(table[0])
    for c in range(1, len(table)):
        value = jnp.where(index == c, jnp.int32(table[c]), value)
    return value


def layer_of_steps(depth):
    if depth == 4:
        mid, end = (1, 2), (0, 3)
        return [
            ("take", 1, None), ("take", 2, mid), ("give", 1, None), ("give", 2, mid), ("expert", 0, None),
            ("expert", 1, None), ("join", 0, None), ("take", 2, end), ("give", 2, end), ("take", 3, mid),
            ("give", 3, mid), ("join", 1, None), ("expert", 2, None), ("take", 3, end), ("give", 3, end),
            ("join", 2, None), ("expert", 3, None), ("join", 3, None),
        ]
    steps = [("expert", 0, None), ("join", 0, None)]
    for k in range(1, depth):
        steps += [("take", k, None), ("give", k, None), ("expert", k, None), ("join", k, None)]
    return steps


def layer_kernel(
    step_ref, route_ref, share_ref, bias_ref, log_ref, skip_ref, x_ref, b_ref, c_ref, gate_ref, resid_ref, wx_ref, wb_ref, wc_ref, ngain_ref, fgain_ref, w_ref,
    sg_ref, su_ref, sd_ref, eg_ref, eu_ref, ed_ref, out_ref,
    step_in, route_in, share_in, bias_in, log_in, skip_in, xin, bin_, cin, gin, rin, wx, wb, wc, ngain, fgain, w_buf, sg_buf, su_buf, sd_buf, eg_buf, eu_buf, ed_buf,
    xh, bh, ch, y_buf, cm_buf, cum_buf, own_last, last_buf, st_buf, f_buf, b_buf, o_buf, c_buf, bef_buf, normed,
    t_buf, info, info_buf, g_buf, x_buf, r_buf, p_buf, q_buf, acc,
    local_sem, h_send, h_recv, l_send, l_recv, f_send, f_recv, b_send, b_recv, o_send, o_recv,
    w_send, w_pass, w_recv, info_send, info_recv, t_send, t_recv, g_send, x_recv, d_send, r_recv, c_send, q_recv,
    *, depth, side, ndp, ways, picks, experts, heads,
):
    tokens, model = t_buf.shape[1:]
    plane, slots = g_buf.shape[1:3]
    groups, wide, state = st_buf.shape
    inner = groups * wide
    per = heads // groups
    width = inner // heads
    share = groups // side
    lanes = plane * slots
    rows = tokens // CHUNKS
    tile = min(512, model)
    sp, dp = lax.axis_index("sp"), lax.axis_index("dp")
    zi, yi = sp // side, sp % side
    me = yi * ndp + dp
    mate = dp + 1 - 2 * (dp % 2)
    order = [[z] + sorted((s for s in range(depth) if s != z), key=lambda s: (abs(s - z), s)) for z in range(depth)]
    source = [pick(zi, [order[z][k] for z in range(depth)]) for k in range(depth)]

    def peer(q):
        return (zi * side + q // ndp, q % ndp)

    def along(step):
        return (sp + step * side, dp)

    def landed(ref, sem):
        pltpu.make_async_copy(ref, ref, sem).wait()

    def remote(src, dst, send, recv, device):
        pltpu.make_async_remote_copy(
            src_ref=src, dst_ref=dst, send_sem=send, recv_sem=recv, device_id=device, device_id_type=MESH
        ).start()

    local = [
        (x_ref, xin), (b_ref, bin_), (c_ref, cin), (wx_ref, wx), (wb_ref, wb), (wc_ref, wc),
        (step_ref, step_in), (route_ref, route_in), (share_ref, share_in), (bias_ref, bias_in), (log_ref, log_in),
        (skip_ref, skip_in),
        (gate_ref, gin), (ngain_ref, ngain), (w_ref, w_buf.at[dp]), (resid_ref, rin), (fgain_ref, fgain),
        (sg_ref, sg_buf), (su_ref, su_buf), (sd_ref, sd_buf),
        (eg_ref.at[0], eg_buf), (eu_ref.at[0], eu_buf), (ed_ref.at[0], ed_buf),
    ]
    loads = [pltpu.make_async_copy(a, b, local_sem.at[i]) for i, (a, b) in enumerate(local)]
    for c in loads:
        c.start()

    barrier = pltpu.get_barrier_semaphore()

    @pl.loop(1, plane)
    def _(j):
        pl.semaphore_signal(barrier, inc=1, device_id=peer((me + j) % plane), device_id_type=MESH)

    @pl.loop(1, depth)
    def _(j):
        pl.semaphore_signal(
            barrier, inc=1, device_id=((zi + j) % depth * side + sp % side, dp), device_id_type=MESH
        )

    for step in (1, ways - 1):
        pl.semaphore_signal(barrier, inc=1, device_id=((sp + step) % ways, dp), device_id_type=MESH)
    pl.semaphore_wait(barrier, plane - 1 + depth - 1 + 2)

    w_rows = w_buf.shape[1]
    piece = w_rows // PARTS
    for hop in range(2, ndp, 2):
        for j in range(PARTS):
            part = pl.ds(j * piece, piece)
            remote(w_ref.at[part], w_buf.at[dp, part], w_send.at[hop // 2], w_recv.at[dp, j], (sp, (dp + hop) % ndp))
    for j in range(PARTS):
        part = pl.ds(j * piece, piece)
        remote(w_ref.at[part], w_buf.at[dp, part], w_send.at[0], w_recv.at[dp, j], (sp, mate))

    for i in range(3):
        loads[i].wait()
    edge = pl.ds(tokens - TAIL, TAIL)

    @pl.when(sp < ways - 1)
    def _():
        for i, (a, b) in enumerate(((xin, xh), (bin_, bh), (cin, ch))):
            remote(a.at[edge], b, h_send.at[i], h_recv.at[i], (sp + 1, dp))

    for i in range(6, 12):
        loads[i].wait()
    raw = step_in[...].astype(F32).T + bias_in[...]
    rate = -jnp.exp(log_in[...])
    skip = skip_in[...]
    step = jnp.maximum(raw, 0.0) + jnp.log(1.0 + jnp.exp(-jnp.abs(raw)))
    logs = step * rate
    row = lax.broadcasted_iota(jnp.int32, (tokens, tokens), 0)
    col = lax.broadcasted_iota(jnp.int32, (tokens, tokens), 1)
    lower = row >= col
    tril = lower.astype(F32)
    cum = lax.dot_general(tril, logs, (((1,), (0,)), ((), ())), precision=HIGH, preferred_element_type=F32)
    cum_t = lax.dot_general(logs, tril, (((0,), (1,)), ((), ())), precision=HIGH, preferred_element_type=F32)
    cum_buf[...] = cum
    last = cum[tokens - 1 : tokens]
    padded = jnp.concatenate([last, jnp.zeros((1, PACK - heads), F32)], axis=1)
    padded = jnp.broadcast_to(padded, (8, PACK))
    own_last[...] = padded
    last_buf[yi] = padded
    to_end = jnp.exp(last - cum)

    @pl.loop(1, side)
    def _(o):
        to = (yi + o) % side
        remote(own_last, last_buf.at[yi], l_send, l_recv.at[yi], (zi * side + to, dp))

    before = jnp.where(row < col, 1.0, 0.0).astype(BF16)
    label = lax.broadcasted_iota(jnp.int32, (experts, tokens), 0).astype(F32)
    lines, used = [], jnp.zeros((experts, 1), F32)
    for p in range(picks):
        named = route_in[p : p + 1].astype(F32)
        hot = jnp.where(label == named, 1.0, 0.0)
        ahead = jnp.dot(hot.astype(BF16), before, preferred_element_type=F32) + used
        used = used + jnp.sum(hot, axis=1, keepdims=True)
        lines.append(named * slots + jnp.sum(ahead * hot, axis=0, keepdims=True))
    lines += [share_in[...], jnp.zeros((8 - 2 * picks, tokens), F32)]
    listed = jnp.concatenate(lines, axis=0)
    info[...] = listed
    info_buf[zi] = listed

    @pl.loop(1, depth)
    def _(j):
        remote(info, info_buf.at[zi], info_send, info_recv.at[zi], ((zi + j) % depth * side + yi, dp))

    for c in loads[3:6]:
        c.wait()

    @pl.when(sp == 0)
    def _():
        for h in (xh, bh, ch):
            h[...] = jnp.zeros(h.shape, BF16)

    @pl.when(sp > 0)
    def _():
        for i, h in enumerate((xh, bh, ch)):
            landed(h, h_recv.at[i])

    turns = [o * share + gl for gl in range(share) for o in range(side)]
    for g in turns:
        xcol = slice(g * wide, (g + 1) * wide)
        bcol = slice(g * state, (g + 1) * state)
        xs = conv_silu(xh[:, xcol], xin[:, xcol], wx[:, xcol])
        bm = conv_silu(bh[:, bcol], bin_[:, bcol], wb[:, bcol]).astype(BF16)
        cm = conv_silu(ch[:, bcol], cin[:, bcol], wc[:, bcol]).astype(BF16)
        cm_buf[:, bcol] = cm
        weighted = xs * spread(step, g * per, per, width)
        ended = (weighted * spread(to_end, g * per, per, width)).astype(BF16)
        fresh = lax.dot_general(ended, bm, (((0,), (0,)), ((), ())), preferred_element_type=F32).astype(BF16)
        st_buf[g] = fresh
        owner, gl = g // share, g % share

        @pl.when(owner != yi)
        def _():
            remote(
                st_buf.at[g], f_buf.at[yi, gl], f_send.at[gl], f_recv.at[yi, gl], (zi * side + owner, dp)
            )

        @pl.when(owner == yi)
        def _():
            f_buf[yi, gl] = fresh

        scores = lax.dot_general(cm, bm, (((1,), (1,)), ((), ())), preferred_element_type=F32)
        scores = jnp.where(lower, scores, 0.0)
        parts = []
        small = weighted.astype(BF16)
        for j in range(per):
            h = g * per + j
            decay = jnp.exp(jnp.minimum(cum[:, h : h + 1] - cum_t[h : h + 1, :], 0.0))
            parts.append(
                jnp.dot((scores * decay).astype(BF16), small[:, j * width : (j + 1) * width],
                        preferred_element_type=F32)
            )
        y_buf[:, xcol] = jnp.concatenate(parts, axis=1) + spread(skip, g * per, per, width) * xs

    @pl.loop(1, side)
    def _(o):
        landed(last_buf.at[(yi + o) % side], l_recv.at[(yi + o) % side])

    head = lax.broadcasted_iota(jnp.int32, (wide, PACK), 0) // width
    lane = lax.broadcasted_iota(jnp.int32, (wide, PACK), 1)
    held = [jnp.exp(last_buf[o, 0:1]) for o in range(side)]
    for gl in range(share):
        g = yi * share + gl
        mine = lane == head + g * per
        factors = [jnp.sum(jnp.where(mine, held[o], 0.0), axis=1, keepdims=True) for o in range(side)]
        for o in range(1, side):
            other = (yi + o) % side
            landed(f_buf.at[other, gl], f_recv.at[other, gl])

        @pl.when(zi == 0)
        def _():
            b_buf[gl] = jnp.zeros((wide, state), BF16)

        @pl.when(zi > 0)
        def _():
            landed(b_buf.at[gl], b_recv.at[gl])

        carry = b_buf[gl].astype(F32)
        for o in range(side):
            o_buf[o, gl] = carry.astype(BF16)
            carry = carry * factors[o] + f_buf[o, gl].astype(F32)
        c_buf[gl] = carry.astype(BF16)

        @pl.when(zi < depth - 1)
        def _():
            remote(c_buf.at[gl], b_buf.at[gl], b_send.at[gl], b_recv.at[gl], along(1))

        for o in range(1, side):
            other = (yi + o) % side
            remote(
                o_buf.at[other, gl], bef_buf.at[g], o_send.at[gl], o_recv.at[g], (zi * side + other, dp)
            )
        bef_buf[g] = o_buf[yi, gl]

    for i in (12, 13):
        loads[i].wait()
    grow = jnp.exp(cum_buf[...])
    for g in turns:
        xcol = slice(g * wide, (g + 1) * wide)

        @pl.when(g // share != yi)
        def _():
            landed(bef_buf.at[g], o_recv.at[g])

        outer = lax.dot_general(
            cm_buf[:, g * state : (g + 1) * state], bef_buf[g], (((1,), (1,)), ((), ())), preferred_element_type=F32
        )
        v = y_buf[:, xcol] + outer * spread(grow, g * per, per, width)
        v = v * silu(gin[:, xcol].astype(F32))
        v = v * lax.rsqrt(jnp.mean(v * v, axis=1, keepdims=True) + EPS)
        normed[:, xcol] = (v * ngain[:, xcol]).astype(BF16)

    for i in range(14, 17):
        loads[i].wait()
    for hop in range(2, ndp, 2):
        held_by = (dp + ndp - hop) % ndp
        for j in range(PARTS):
            part = pl.ds(j * piece, piece)
            landed(w_buf.at[held_by, part], w_recv.at[held_by, j])
            remote(
                w_buf.at[held_by, part], w_buf.at[held_by, part], w_pass.at[hop // 2], w_recv.at[held_by, j], (sp, mate)
            )
    for hop in range(0, ndp, 2):
        held_by = (mate + ndp - hop) % ndp
        for j in range(PARTS):
            landed(w_buf.at[held_by, pl.ds(j * piece, piece)], w_recv.at[held_by, j])
    square = jnp.zeros((tokens, 1), F32)
    for n in range(0, model, tile):
        cols = slice(n, n + tile)
        total = rin[:, cols].astype(F32)
        for i in range(ndp):
            total = total + jnp.dot(
                normed[:, i * w_rows : (i + 1) * w_rows], w_buf[i, :, cols], preferred_element_type=F32
            )
        total = total.astype(BF16).astype(F32)
        acc[:, cols] = total
        square = square + jnp.sum(total * total, axis=1, keepdims=True)
    scale = lax.rsqrt(square / model + EPS)
    for n in range(0, model, tile):
        cols = slice(n, n + tile)
        t_buf[zi, :, cols] = (acc[:, cols] * scale * fgain[:, cols]).astype(BF16)

    def token_copy(s, j, up):
        part = pl.ds(j * rows, rows)
        return pltpu.make_async_remote_copy(
            src_ref=t_buf.at[s, part], dst_ref=t_buf.at[s, part], send_sem=t_send.at[1 if up else 0, s],
            recv_sem=t_recv.at[s, j], device_id=along(1 if up else -1), device_id_type=MESH,
        )

    def sum_copy(s, j, up):
        part = pl.ds(j * rows, rows)
        into = s if up else jnp.where(s == zi - 1, depth, s)
        return pltpu.make_async_remote_copy(
            src_ref=p_buf.at[s, part], dst_ref=q_buf.at[into, part], send_sem=c_send.at[s],
            recv_sem=q_recv.at[into, j], device_id=along(1 if up else -1), device_id_type=MESH,
        )

    def send_sum(s, j):
        @pl.when(s > zi)
        def _():
            sum_copy(s, j, True).start()

        @pl.when(s < zi)
        def _():
            sum_copy(s, j, False).start()

    def send_tokens(s, j):
        @pl.when((s <= zi) & (zi < depth - 1))
        def _():
            token_copy(s, j, True).start()

        @pl.when((s >= zi) & (zi > 0))
        def _():
            token_copy(s, j, False).start()

    def take(k):
        s = source[k]
        landed(info_buf.at[s], info_recv.at[s])
        for j in range(CHUNKS):
            landed(t_buf.at[s, pl.ds(j * rows, rows)], t_recv.at[s, j])
            send_tokens(s, j)

    def target():
        row = lax.broadcasted_iota(jnp.int32, (lanes, tokens), 0) + zi * lanes
        return row.astype(F32)

    def give(k):
        s = source[k]
        listing = info_buf[s]
        slot = target()
        chosen = slot == listing[0:1]
        for p in range(1, picks):
            chosen = chosen | (slot == listing[p : p + 1])
        chosen = jnp.where(chosen, 1.0, 0.0).astype(BF16)
        for n in range(0, model, tile):
            cols = slice(n, n + tile)
            part = jnp.dot(chosen, t_buf[s, :, cols], preferred_element_type=F32).astype(BF16)
            g_buf[s, :, :, cols] = part.reshape(plane, slots, tile)

        @pl.loop(1, plane)
        def _(j):
            q = (me + j) % plane
            pltpu.make_async_remote_copy(
                src_ref=g_buf.at[s, q], dst_ref=x_buf.at[s, me], send_sem=g_send.at[s], recv_sem=x_recv.at[s],
                device_id=peer(q), device_id_type=MESH,
            ).start()

        x_buf[s, me] = g_buf[s, me]

    def expert(k):
        s = source[k]
        if k == 0:
            for c in loads[20:]:
                c.wait()
        landed(x_buf.at[s, pl.ds(0, plane - 1)], x_recv.at[s])
        rows_in = x_buf[s].reshape(lanes, model)
        gate = jnp.dot(rows_in, eg_buf[...], preferred_element_type=F32)
        up = jnp.dot(rows_in, eu_buf[...], preferred_element_type=F32)
        hidden = (silu(gate) * up).astype(BF16)
        for n in range(0, model, tile):
            cols = slice(n, n + tile)
            part = jnp.dot(hidden, ed_buf[:, cols], preferred_element_type=F32).astype(BF16)
            x_buf[s, :, :, cols] = part.reshape(plane, slots, tile)

        @pl.loop(1, plane)
        def _(j):
            q = (me + j) % plane
            pltpu.make_async_remote_copy(
                src_ref=x_buf.at[s, q], dst_ref=r_buf.at[s, me], send_sem=d_send.at[s], recv_sem=r_recv.at[s],
                device_id=peer(q), device_id_type=MESH,
            ).start()

        r_buf[s, me] = x_buf[s, me]

    def join(k):
        s = source[k]
        landed(r_buf.at[s, pl.ds(0, plane - 1)], r_recv.at[s])
        listing = info_buf[s]
        slot = target()
        weight = jnp.zeros((lanes, tokens), F32)
        for p in range(picks):
            weight = weight + jnp.where(slot == listing[p : p + 1], listing[picks + p : picks + p + 1], 0.0)
        high = weight.astype(BF16)
        low = (weight - high.astype(F32)).astype(BF16)
        for n in range(0, model, tile):
            cols = slice(n, n + tile)
            block = r_buf[s, :, :, cols].reshape(lanes, tile)
            part = lax.dot_general(high, block, (((0,), (0,)), ((), ())), preferred_element_type=F32)
            part = part + lax.dot_general(low, block, (((0,), (0,)), ((), ())), preferred_element_type=F32)
            if k == 0:
                acc[:, cols] = acc[:, cols] + part
            else:
                p_buf[s, :, cols] = part.astype(BF16)
        if k:
            @pl.when((zi == 0) | (zi == depth - 1))
            def _():
                for j in range(CHUNKS):
                    send_sum(s, j)

    for j in range(CHUNKS):
        send_tokens(source[0], j)
    give(0)

    for c in loads[17:20]:
        c.wait()
    x = t_buf[zi]
    hidden = silu(jnp.dot(x, sg_buf[...], preferred_element_type=F32)) * jnp.dot(
        x, su_buf[...], preferred_element_type=F32
    )
    hidden = hidden.astype(BF16)
    for n in range(0, model, tile):
        cols = slice(n, n + tile)
        acc[:, cols] = acc[:, cols] + jnp.dot(hidden, sd_buf[:, cols], preferred_element_type=F32)

    actions = {"take": take, "give": give, "expert": expert, "join": join}
    for name, k, planes in layer_of_steps(depth):
        if planes is None:
            actions[name](k)
        else:
            taken = zi == planes[0]
            for z in planes[1:]:
                taken = taken | (zi == z)

            @pl.when(taken)
            def _(name=name, k=k):
                actions[name](k)

    def far(z, s):
        return depth - 1 - s + depth - 1 - z if s < z else s + z

    passing = [sorted((s for s in range(depth) if s != z), key=lambda s, z=z: (far(z, s), s)) for z in range(depth)]

    @pl.when((zi > 0) & (zi < depth - 1))
    def _():
        for i in range(depth - 1):
            s = pick(zi, [passing[z][i] for z in range(depth)])
            for j in range(CHUNKS):
                part = pl.ds(j * rows, rows)
                landed(q_buf.at[s, part], q_recv.at[s, j])
                p_buf[s, part] = (p_buf[s, part].astype(F32) + q_buf[s, part].astype(F32)).astype(BF16)
                send_sum(s, j)

    for j in range(CHUNKS):
        part = pl.ds(j * rows, rows)

        @pl.when(zi > 0)
        def _():
            landed(q_buf.at[zi, part], q_recv.at[zi, j])
            acc[part] = acc[part] + q_buf[zi, part].astype(F32)

        @pl.when(zi < depth - 1)
        def _():
            landed(q_buf.at[depth, part], q_recv.at[depth, j])
            acc[part] = acc[part] + q_buf[depth, part].astype(F32)

        out_ref[part] = acc[part].astype(BF16)

    @pl.loop(1, depth)
    def _(j):
        landed(info, info_send)

    @pl.loop(1, side)
    def _(o):
        landed(own_last, l_send)

    @pl.when(sp < ways - 1)
    def _():
        for i, h in enumerate((xh, bh, ch)):
            landed(h, h_send.at[i])

    for gl in range(share):
        for _ in range(1, side):
            landed(st_buf.at[0], f_send.at[gl])
            landed(st_buf.at[0], o_send.at[gl])

        @pl.when(zi < depth - 1)
        def _():
            landed(c_buf.at[gl], b_send.at[gl])

    for hop in range(0, ndp, 2):
        landed(w_buf.at[0], w_send.at[hop // 2])
        if hop:
            landed(w_buf.at[0], w_pass.at[hop // 2])

    for k in range(depth):
        s = source[k]
        landed(g_buf.at[s, pl.ds(0, plane - 1)], g_send.at[s])
        landed(x_buf.at[s, pl.ds(0, plane - 1)], d_send.at[s])
        if k:
            landed(p_buf.at[s], c_send.at[s])

        @pl.when((s <= zi) & (zi < depth - 1))
        def _():
            landed(t_buf.at[s], t_send.at[1, s])

        @pl.when((s >= zi) & (zi > 0))
        def _():
            landed(t_buf.at[s], t_send.at[0, s])


def vmem(count):
    return [pl.BlockSpec(memory_space=pltpu.VMEM)] * count


def body(
    residual, head_input, gate_input, b_input, c_input, step_input, conv_weight, conv_b_weight,
    conv_c_weight, step_bias, decay_log, skip, norm_gain, out_weight, ffn_gain, shared_gate,
    shared_up, shared_down, expert_gate, expert_up, expert_down, routes, route_weights,
):
    tokens, inner = head_input.shape[1:]
    heads = step_bias.shape[0]
    state = 128
    span = b_input.shape[2]
    groups = span // state
    model = residual.shape[2]
    ways, ndp = lax.axis_size("sp"), lax.axis_size("dp")
    picks = routes.shape[2]
    side = max(1, ndp // 2)
    depth = ways // side
    plane = side * ndp
    experts = ways * ndp
    slots = max(16, 2 * tokens * picks // experts)
    share = groups // side
    wide = inner // groups
    hbm = [pl.BlockSpec(memory_space=pl.ANY)]
    dma = pltpu.SemaphoreType.DMA
    hidden = expert_gate.shape[2]
    shared = shared_gate.shape[1]

    def halves(*shape):
        return pltpu.VMEM(shape, BF16)

    def floats(*shape):
        return pltpu.VMEM(shape, F32)

    out = pl.pallas_call(
        lambda *refs: layer_kernel(
            *refs, depth=depth, side=side, ndp=ndp, ways=ways, picks=picks, experts=experts, heads=heads
        ),
        out_shape=jax.ShapeDtypeStruct((tokens, model), BF16),
        in_specs=hbm * 23,
        out_specs=vmem(1)[0],
        scratch_shapes=[
            halves(heads, tokens), pltpu.VMEM((picks, tokens), jnp.int32), floats(picks, tokens), floats(1, heads),
            floats(1, heads), floats(1, heads), halves(tokens, inner), halves(tokens, span), halves(tokens, span),
            halves(tokens, inner), halves(tokens, model), halves(*conv_weight.shape), halves(*conv_b_weight.shape),
            halves(*conv_c_weight.shape), floats(1, inner), floats(1, model),
            halves(ndp, inner // ndp, model), halves(model, shared), halves(model, shared), halves(shared, model),
            halves(model, hidden), halves(model, hidden), halves(hidden, model),
            halves(TAIL, inner), halves(TAIL, span), halves(TAIL, span), floats(tokens, inner), halves(tokens, span),
            floats(tokens, heads), floats(8, PACK), floats(side, 8, PACK), halves(groups, wide, state),
            halves(side, share, wide, state), halves(share, wide, state), halves(side, share, wide, state),
            halves(share, wide, state), halves(groups, wide, state), halves(tokens, inner),
            halves(depth, tokens, model), floats(8, tokens), floats(depth, 8, tokens),
            halves(depth, plane, slots, model), halves(depth, plane, slots, model), halves(depth, plane, slots, model),
            halves(depth, tokens, model), halves(depth + 1, tokens, model), floats(tokens, model),
            dma((23,)), dma((3,)), dma((3,)), dma, dma((side,)), dma((share,)), dma((side, share)), dma((share,)),
            dma((share,)), dma((share,)), dma((groups,)), dma((max(1, ndp // 2),)), dma((max(1, ndp // 2),)),
            dma((ndp, PARTS)),
            dma, dma((depth,)), dma((2, depth)), dma((depth, CHUNKS)), dma((depth,)), dma((depth,)),
            dma((depth,)), dma((depth,)), dma((depth,)), dma((depth + 1, CHUNKS)),
        ],
        compiler_params=pltpu.CompilerParams(
            vmem_limit_bytes=63 * 1024 * 1024, collective_id=1, has_side_effects=True
        ),
        cost_estimate=pl.CostEstimate(flops=8_000_000_000, bytes_accessed=24_000_000, transcendentals=500_000),
    )(
        step_input[0].T, routes[0].T, route_weights[0].T, step_bias[None], decay_log[None], skip[None], head_input[0], b_input[0], c_input[0], gate_input[0], residual[0], conv_weight, conv_b_weight,
        conv_c_weight, norm_gain[None], ffn_gain[None], out_weight, shared_gate, shared_up, shared_down,
        expert_gate, expert_up, expert_down,
    )
    return out[None]


def solution(mesh):
    rows = P("dp", "sp", None)
    split = P(("sp", "dp"), None, None)
    return jax.shard_map(
        body,
        mesh=mesh,
        in_specs=(rows,) * 6 + (P(),) * 7 + (P("dp", None),) + (P(),) * 4 + (split,) * 3 + (rows,) * 2,
        out_specs=rows,
        check_vma=False,
    )
```

time: 177 us -> 148 us (0.84)
  Pallas kernels: 105 us -> 146 us
  waiting for transfers between devices: 23.1 us -> 0 us
  blocking collectives: 21.4 us -> 0 us
  between operations: 13.6 us -> 0.01 us
  starting transfers between devices: 8.43 us -> 0 us
  local copies, waits for them, and re-layouts: 3.95 us -> 1.88 us
    pallas_call x4 -> x1, Pallas kernels: 105 us -> 146 us  [body(): pl.pallas_call(lambda *refs: layer_kernel(*refs, depth=depth, side=side,...]
    all_to_all x1 -> x0, blocking collectives: 21.4 us -> none  [body(): lax.all_to_all(states, 'sp', split_axis=0, concat_axis=0, tiled=True)]
    all_to_all x1 -> x0, waiting for transfers between devices: 12 us -> none  [body(): lax.all_to_all(prefix, 'sp', split_axis=0, concat_axis=0, tiled=True)]
    all_gather x1 -> x0, waiting for transfers between devices: 8.86 us -> none  [body(): weight = lax.all_gather(out_weight, 'dp', axis=0, tiled=True)]
    ppermute x1 -> x0, starting transfers between devices: 4.9 us -> none  [body(): halo = lax.ppermute(tail, 'sp', [(i, i + 1) for i in range(ways - 1)])]
    all_to_all x1 -> x0, starting transfers between devices: 3.49 us -> none  [body(): lax.all_to_all(prefix, 'sp', split_axis=0, concat_axis=0, tiled=True)]
  transfers between devices with their start and end apart: 3 -> 0, of which waited for: 3 -> 0; matrix products, arithmetic and copies ran while one was open for 1% -> 0% of each run, Pallas kernels for 4% -> 0%
where the time goes in v2:
time: 148 us
  Pallas kernels  146 us (99%)
  local copies, waits for them, and re-layouts  1.88 us (1%)
    pallas_call x1, Pallas kernels, body(): pl.pallas_call(lambda *refs: layer_kernel(*refs, depth=depth, side=side,...  146 us

profile of v2, /device:TPU:0, one launch (start us, length us, event | category | flops | bytes accessed | tf_op | source)
XLA Modules:
  0.0 147.9 jit_solution(13641058912852397043)
XLA Ops:
  0.0 146.0 %shard_map.217 = bf16[128,2048]{1,0:T(8,128)(2,1)} custom-call(bf16[32,128]{1,0:T(8,128)(2,1)} %bitcast.26, s32[2,128]{1,0:T(2,128)} %bitcast.29, f32[2,128]{1,0:T(2,128)} %bitcast.30, f32[1,32]{1,0:T(1,128)} %bitcast.31, f32[1,32]{1,0:T(1,128)} %bitcast.32, f32[1,32]{1,0:T(1,128)} %bitcast.33, bf16[128,2048]{1,0:T(8,128)(2,1)} %bitcast.21, ...), custom_call_target="tpu_custom_call" | custom-call | flops 8000000000 | bytes 24000000 | tf_op jit(solution)/shard_map/pallas_call | solution.py:589
  146.0 1.9 %copy.25 = bf16[1,128,2048]{2,1,0:T(8,128)(2,1)} copy(bf16[1,128,2048]{2,1,0:T(8,128)(2,1)} %bitcast.20) | data formatting | bytes 1048576

commit v3 on v2

--- a/solution.py
+++ b/solution.py
@@ -13,8 +13,8 @@
 F32 = jnp.float32
 BF16 = jnp.bfloat16
 MESH = pl.DeviceIdType.MESH
-CHUNKS = 4
-PARTS = 4
+CHUNKS = 8
+PARTS = 16
 
 
 def silu(v):
@@ -48,14 +48,21 @@
     return value
 
 
+def orders(depth):
+    if depth == 4:
+        return [[0, 1, 3, 2], [1, 0, 2, 3], [2, 3, 1, 0], [3, 2, 0, 1]]
+    return [[z] + sorted((s for s in range(depth) if s != z), key=lambda s: (abs(s - z), s)) for z in range(depth)]
+
+
 def layer_of_steps(depth):
     if depth == 4:
         mid, end = (1, 2), (0, 3)
         return [
-            ("take", 1, None), ("take", 2, mid), ("give", 1, None), ("give", 2, mid), ("expert", 0, None),
-            ("expert", 1, None), ("join", 0, None), ("take", 2, end), ("give", 2, end), ("take", 3, mid),
-            ("give", 3, mid), ("join", 1, None), ("expert", 2, None), ("take", 3, end), ("give", 3, end),
-            ("join", 2, None), ("expert", 3, None), ("join", 3, None),
+            ("expert", 0, None), ("take", 1, end), ("pair", 1, mid), ("give", 1, None),
+            ("give", 2, mid), ("join", 0, end), ("take", 3, mid), ("late", 2, mid), ("expert", 1, None),
+            ("give", 3, mid), ("join", 0, mid), ("take", 2, end), ("give", 2, end), ("join", 1, None),
+            ("expert", 2, None), ("take", 3, end), ("give", 3, end), ("join", 2, None), ("expert", 3, None),
+            ("join", 3, None),
         ]
     steps = [("expert", 0, None), ("join", 0, None)]
     for k in range(1, depth):
@@ -70,7 +77,7 @@
     xh, bh, ch, y_buf, cm_buf, cum_buf, own_last, last_buf, st_buf, f_buf, b_buf, o_buf, c_buf, bef_buf, normed,
     t_buf, info, info_buf, g_buf, x_buf, r_buf, p_buf, q_buf, acc,
     local_sem, h_send, h_recv, l_send, l_recv, f_send, f_recv, b_send, b_recv, o_send, o_recv,
-    w_send, w_pass, w_recv, info_send, info_recv, t_send, t_recv, g_send, x_recv, d_send, r_recv, c_send, q_recv,
+    w_send, w_pass, w_near, w_recv, m_recv, info_send, info_recv, t_send, t_recv, g_send, x_recv, d_send, r_recv, c_send, q_recv,
     *, depth, side, ndp, ways, picks, experts, heads,
 ):
     tokens, model = t_buf.shape[1:]
@@ -87,7 +94,7 @@
     zi, yi = sp // side, sp % side
     me = yi * ndp + dp
     mate = dp + 1 - 2 * (dp % 2)
-    order = [[z] + sorted((s for s in range(depth) if s != z), key=lambda s: (abs(s - z), s)) for z in range(depth)]
+    order = orders(depth)
     source = [pick(zi, [order[z][k] for z in range(depth)]) for k in range(depth)]
 
     def peer(q):
@@ -134,13 +141,44 @@
 
     w_rows = w_buf.shape[1]
     piece = w_rows // PARTS
-    for hop in range(2, ndp, 2):
-        for j in range(PARTS):
-            part = pl.ds(j * piece, piece)
-            remote(w_ref.at[part], w_buf.at[dp, part], w_send.at[hop // 2], w_recv.at[dp, j], (sp, (dp + hop) % ndp))
-    for j in range(PARTS):
-        part = pl.ds(j * piece, piece)
-        remote(w_ref.at[part], w_buf.at[dp, part], w_send.at[0], w_recv.at[dp, j], (sp, mate))
+    quarter = PARTS // 4
+    half = (yi + zi) % 2
+
+    def place(which, i):
+        return which * 2 * quarter + (i % 2) * quarter + i // 2
+
+    def span_of(n):
+        return pl.ds(pl.multiple_of(n * piece, piece), piece)
+
+    for i in range(2 * quarter):
+        n = place(half, i)
+        for hop in range(2, ndp, 2):
+            remote(
+                w_ref.at[span_of(n)], w_buf.at[dp, span_of(n)], w_send.at[hop // 2], w_recv.at[dp, n],
+                (sp, (dp + hop) % ndp),
+            )
+    remote(w_ref, w_buf.at[dp], w_send.at[0], m_recv.at[dp], (sp, mate))
+    near = (zi * side + yi + 1 - 2 * (yi % 2), sp + (1 - 2 * (zi % 2)) * side)
+
+    def pass_on(held_by, n):
+        part = w_buf.at[held_by, span_of(n)]
+        remote(part, part, w_pass.at[held_by], w_recv.at[held_by, n], (sp, mate))
+
+    def relay(i):
+        n = place(half, i)
+        for hop in range(2, ndp, 2):
+            held_by = (dp + ndp - hop) % ndp
+            part = w_buf.at[held_by, span_of(n)]
+            landed(part, w_recv.at[held_by, n])
+            remote(part, part, w_near.at[i % 2, held_by], w_recv.at[held_by, n], (near[i % 2], dp))
+            pass_on(held_by, n)
+
+    def receive(i):
+        n = place(1 - half, i)
+        for hop in range(2, ndp, 2):
+            held_by = (dp + ndp - hop) % ndp
+            landed(w_buf.at[held_by, span_of(n)], w_recv.at[held_by, n])
+            pass_on(held_by, n)
 
     for i in range(3):
         loads[i].wait()
@@ -208,8 +246,11 @@
         for i, h in enumerate((xh, bh, ch)):
             landed(h, h_recv.at[i])
 
+    relay(0)
     turns = [o * share + gl for gl in range(share) for o in range(side)]
     for g in turns:
+        if g == turns[groups // 2]:
+            relay(1)
         xcol = slice(g * wide, (g + 1) * wide)
         bcol = slice(g * state, (g + 1) * state)
         xs = conv_silu(xh[:, xcol], xin[:, xcol], wx[:, xcol])
@@ -245,6 +286,12 @@
             )
         y_buf[:, xcol] = jnp.concatenate(parts, axis=1) + spread(skip, g * per, per, width) * xs
 
+    relay(2)
+    for i in (3, 4, 5):
+        @pl.when(zi >= i // 2 - i // 4)
+        def _():
+            relay(i)
+
     @pl.loop(1, side)
     def _(o):
         landed(last_buf.at[(yi + o) % side], l_recv.at[(yi + o) % side])
@@ -287,9 +334,18 @@
 
     for i in (12, 13):
         loads[i].wait()
+    for i in (3, 4, 5):
+        @pl.when(zi < i // 2 - i // 4)
+        def _():
+            relay(i)
+
     grow = jnp.exp(cum_buf[...])
     for g in turns:
         xcol = slice(g * wide, (g + 1) * wide)
+        if g == turns[groups // 4]:
+            relay(6)
+        if g == turns[3 * groups // 4]:
+            relay(7)
 
         @pl.when(g // share != yi)
         def _():
@@ -305,26 +361,30 @@
 
     for i in range(14, 17):
         loads[i].wait()
+    receive(0)
+    receive(1)
+    landed(w_buf.at[mate], m_recv.at[mate])
+
+    def product(i, cols):
+        start = pl.multiple_of(i * w_rows, w_rows)
+        return jnp.dot(normed[:, pl.ds(start, w_rows)], w_buf[i, :, cols], preferred_element_type=F32)
+
+    for n in range(0, model, tile):
+        cols = slice(n, n + tile)
+        acc[:, cols] = rin[:, cols].astype(F32) + product(dp, cols) + product(mate, cols)
+    for i in range(2, 2 * quarter):
+        receive(i)
+    away = []
     for hop in range(2, ndp, 2):
-        held_by = (dp + ndp - hop) % ndp
-        for j in range(PARTS):
-            part = pl.ds(j * piece, piece)
-            landed(w_buf.at[held_by, part], w_recv.at[held_by, j])
-            remote(
-                w_buf.at[held_by, part], w_buf.at[held_by, part], w_pass.at[hop // 2], w_recv.at[held_by, j], (sp, mate)
-            )
-    for hop in range(0, ndp, 2):
-        held_by = (mate + ndp - hop) % ndp
-        for j in range(PARTS):
-            landed(w_buf.at[held_by, pl.ds(j * piece, piece)], w_recv.at[held_by, j])
+        away += [(dp + ndp - hop) % ndp, (mate + ndp - hop) % ndp]
+        for n in range(PARTS):
+            landed(w_buf.at[away[-1], span_of(n)], w_recv.at[away[-1], n])
     square = jnp.zeros((tokens, 1), F32)
     for n in range(0, model, tile):
         cols = slice(n, n + tile)
-        total = rin[:, cols].astype(F32)
-        for i in range(ndp):
-            total = total + jnp.dot(
-                normed[:, i * w_rows : (i + 1) * w_rows], w_buf[i, :, cols], preferred_element_type=F32
-            )
+        total = acc[:, cols]
+        for i in away:
+            total = total + product(i, cols)
         total = total.astype(BF16).astype(F32)
         acc[:, cols] = total
         square = square + jnp.sum(total * total, axis=1, keepdims=True)
@@ -357,14 +417,19 @@
         def _():
             sum_copy(s, j, False).start()
 
+    def send_up(s, j):
+        @pl.when((s <= zi) & (zi < depth - 1))
+        def _():
+            token_copy(s, j, True).start()
+
+    def send_down(s, j):
+        @pl.when((s >= zi) & (zi > 0))
+        def _():
+            token_copy(s, j, False).start()
+
     def send_tokens(s, j):
-        @pl.when((s <= zi) & (zi < depth - 1))
-        def _():
-            token_copy(s, j, True).start()
-
-        @pl.when((s >= zi) & (zi > 0))
-        def _():
-            token_copy(s, j, False).start()
+        send_up(s, j)
+        send_down(s, j)
 
     def take(k):
         s = source[k]
@@ -372,6 +437,20 @@
         for j in range(CHUNKS):
             landed(t_buf.at[s, pl.ds(j * rows, rows)], t_recv.at[s, j])
             send_tokens(s, j)
+
+    lag = 3 * CHUNKS // 8
+
+    def pair(k):
+        for s in (source[k], source[k + 1]):
+            landed(info_buf.at[s], info_recv.at[s])
+        for j in range(CHUNKS):
+            for s in (source[k], source[k + 1]):
+                landed(t_buf.at[s, pl.ds(j * rows, rows)], t_recv.at[s, j])
+            send_tokens(source[k], j)
+
+    def late(k):
+        for j in range(CHUNKS):
+            send_tokens(source[k], j)
 
     def target():
         row = lax.broadcasted_iota(jnp.int32, (lanes, tokens), 0) + zi * lanes
@@ -402,9 +481,6 @@
 
     def expert(k):
         s = source[k]
-        if k == 0:
-            for c in loads[20:]:
-                c.wait()
         landed(x_buf.at[s, pl.ds(0, plane - 1)], x_recv.at[s])
         rows_in = x_buf[s].reshape(lanes, model)
         gate = jnp.dot(rows_in, eg_buf[...], preferred_element_type=F32)
@@ -451,7 +527,7 @@
                     send_sum(s, j)
 
     for j in range(CHUNKS):
-        send_tokens(source[0], j)
+        send_tokens(zi, j)
     give(0)
 
     for c in loads[17:20]:
@@ -465,7 +541,10 @@
         cols = slice(n, n + tile)
         acc[:, cols] = acc[:, cols] + jnp.dot(hidden, sd_buf[:, cols], preferred_element_type=F32)
 
-    actions = {"take": take, "give": give, "expert": expert, "join": join}
+    for c in loads[20:]:
+        c.wait()
+
+    actions = {"take": take, "pair": pair, "late": late, "give": give, "expert": expert, "join": join}
     for name, k, planes in layer_of_steps(depth):
         if planes is None:
             actions[name](k)
@@ -478,20 +557,33 @@
             def _(name=name, k=k):
                 actions[name](k)
 
+    def pass_sum(s, j):
+        part = pl.ds(j * rows, rows)
+        landed(q_buf.at[s, part], q_recv.at[s, j])
+        p_buf[s, part] = (p_buf[s, part].astype(F32) + q_buf[s, part].astype(F32)).astype(BF16)
+        send_sum(s, j)
+
     def far(z, s):
         return depth - 1 - s + depth - 1 - z if s < z else s + z
 
-    passing = [sorted((s for s in range(depth) if s != z), key=lambda s, z=z: (far(z, s), s)) for z in range(depth)]
-
     @pl.when((zi > 0) & (zi < depth - 1))
     def _():
-        for i in range(depth - 1):
-            s = pick(zi, [passing[z][i] for z in range(depth)])
+        if depth == 4:
+            first, second, third = [pick(zi, [0] + t + [0]) for t in ([3, 0], [0, 3], [2, 1])]
+            for j in range(CHUNKS + lag):
+                if j < CHUNKS:
+                    pass_sum(first, j)
+                if j >= lag:
+                    pass_sum(second, j - lag)
             for j in range(CHUNKS):
-                part = pl.ds(j * rows, rows)
-                landed(q_buf.at[s, part], q_recv.at[s, j])
-                p_buf[s, part] = (p_buf[s, part].astype(F32) + q_buf[s, part].astype(F32)).astype(BF16)
-                send_sum(s, j)
+                pass_sum(third, j)
+        else:
+            passing = [
+                sorted((s for s in range(depth) if s != z), key=lambda s, z=z: (far(z, s), s)) for z in range(depth)
+            ]
+            for i in range(depth - 1):
+                for j in range(CHUNKS):
+                    pass_sum(pick(zi, [passing[z][i] for z in range(depth)]), j)
 
     for j in range(CHUNKS):
         part = pl.ds(j * rows, rows)
@@ -530,10 +622,13 @@
         def _():
             landed(c_buf.at[gl], b_send.at[gl])
 
-    for hop in range(0, ndp, 2):
-        landed(w_buf.at[0], w_send.at[hop // 2])
-        if hop:
-            landed(w_buf.at[0], w_pass.at[hop // 2])
+    landed(w_buf.at[0], w_send.at[0])
+    for hop in range(2, ndp, 2):
+        held_by = (dp + ndp - hop) % ndp
+        landed(w_buf.at[0, pl.ds(0, 2 * quarter * piece)], w_send.at[hop // 2])
+        landed(w_buf.at[0], w_pass.at[held_by])
+        for i in range(2):
+            landed(w_buf.at[0, pl.ds(0, quarter * piece)], w_near.at[i, held_by])
 
     for k in range(depth):
         s = source[k]
@@ -608,8 +703,8 @@
             halves(depth, plane, slots, model), halves(depth, plane, slots, model), halves(depth, plane, slots, model),
             halves(depth, tokens, model), halves(depth + 1, tokens, model), floats(tokens, model),
             dma((23,)), dma((3,)), dma((3,)), dma, dma((side,)), dma((share,)), dma((side, share)), dma((share,)),
-            dma((share,)), dma((share,)), dma((groups,)), dma((max(1, ndp // 2),)), dma((max(1, ndp // 2),)),
-            dma((ndp, PARTS)),
+            dma((share,)), dma((share,)), dma((groups,)), dma((max(1, ndp // 2),)), dma((ndp,)),
+            dma((2, ndp)), dma((ndp, PARTS)), dma((ndp,)),
             dma, dma((depth,)), dma((2, depth)), dma((depth, CHUNKS)), dma((depth,)), dma((depth,)),
             dma((depth,)), dma((depth,)), dma((depth,)), dma((depth + 1, CHUNKS)),
         ],

time: 148 us -> 128 us (0.86)
  the two profiles are of different devices: /device:TPU:0 before, /device:TPU:17 now
where the time goes in v3:
time: 128 us; the launch traced here: 127 us
  Pallas kernels  126 us (98%)
  local copies, waits for them, and re-layouts  1.88 us (1%)
    pallas_call x1, Pallas kernels, body(): pl.pallas_call(lambda *refs: layer_kernel(*refs, depth=depth, side=side,...  126 us

profile of v3, /device:TPU:17, one launch (start us, length us, event | category | flops | bytes accessed | tf_op | source)
XLA Modules:
  0.0 127.4 jit_solution(14940598537083760233)
XLA Ops:
  0.0 125.5 %shard_map.217 = bf16[128,2048]{1,0:T(8,128)(2,1)} custom-call(bf16[32,128]{1,0:T(8,128)(2,1)} %bitcast.26, s32[2,128]{1,0:T(2,128)} %bitcast.29, f32[2,128]{1,0:T(2,128)} %bitcast.30, f32[1,32]{1,0:T(1,128)} %bitcast.31, f32[1,32]{1,0:T(1,128)} %bitcast.32, f32[1,32]{1,0:T(1,128)} %bitcast.33, bf16[128,2048]{1,0:T(8,128)(2,1)} %bitcast.21, ...), custom_call_target="tpu_custom_call" | custom-call | flops 8000000000 | bytes 24000000 | tf_op jit(solution)/shard_map/pallas_call | solution.py:684
  125.5 1.9 %copy.25 = bf16[1,128,2048]{2,1,0:T(8,128)(2,1)} copy(bf16[1,128,2048]{2,1,0:T(8,128)(2,1)} %bitcast.20) | data formatting | bytes 1048576

commit v4 on v3

--- a/solution.py
+++ b/solution.py
@@ -74,7 +74,7 @@
     step_ref, route_ref, share_ref, bias_ref, log_ref, skip_ref, x_ref, b_ref, c_ref, gate_ref, resid_ref, wx_ref, wb_ref, wc_ref, ngain_ref, fgain_ref, w_ref,
     sg_ref, su_ref, sd_ref, eg_ref, eu_ref, ed_ref, out_ref,
     step_in, route_in, share_in, bias_in, log_in, skip_in, xin, bin_, cin, gin, rin, wx, wb, wc, ngain, fgain, w_buf, sg_buf, su_buf, sd_buf, eg_buf, eu_buf, ed_buf,
-    xh, bh, ch, y_buf, cm_buf, cum_buf, own_last, last_buf, st_buf, f_buf, b_buf, o_buf, c_buf, bef_buf, normed,
+    xh, bh, ch, y_buf, cm_buf, bm_buf, small_buf, cum_buf, own_last, last_buf, st_buf, f_buf, b_buf, o_buf, c_buf, bef_buf, normed,
     t_buf, info, info_buf, g_buf, x_buf, r_buf, p_buf, q_buf, acc,
     local_sem, h_send, h_recv, l_send, l_recv, f_send, f_recv, b_send, b_recv, o_send, o_recv,
     w_send, w_pass, w_near, w_recv, m_recv, info_send, info_recv, t_send, t_recv, g_send, x_recv, d_send, r_recv, c_send, q_recv,
@@ -258,6 +258,9 @@
         cm = conv_silu(ch[:, bcol], cin[:, bcol], wc[:, bcol]).astype(BF16)
         cm_buf[:, bcol] = cm
         weighted = xs * spread(step, g * per, per, width)
+        y_buf[:, xcol] = xs
+        bm_buf[:, bcol] = bm
+        small_buf[:, xcol] = weighted.astype(BF16)
         ended = (weighted * spread(to_end, g * per, per, width)).astype(BF16)
         fresh = lax.dot_general(ended, bm, (((0,), (0,)), ((), ())), preferred_element_type=F32).astype(BF16)
         st_buf[g] = fresh
@@ -273,22 +276,31 @@
         def _():
             f_buf[yi, gl] = fresh
 
-        scores = lax.dot_general(cm, bm, (((1,), (1,)), ((), ())), preferred_element_type=F32)
-        scores = jnp.where(lower, scores, 0.0)
-        parts = []
-        small = weighted.astype(BF16)
-        for j in range(per):
-            h = g * per + j
-            decay = jnp.exp(jnp.minimum(cum[:, h : h + 1] - cum_t[h : h + 1, :], 0.0))
-            parts.append(
-                jnp.dot((scores * decay).astype(BF16), small[:, j * width : (j + 1) * width],
-                        preferred_element_type=F32)
+    def inside():
+        for g in turns:
+            xcol = slice(g * wide, (g + 1) * wide)
+            bcol = slice(g * state, (g + 1) * state)
+            scores = lax.dot_general(
+                cm_buf[:, bcol], bm_buf[:, bcol], (((1,), (1,)), ((), ())), preferred_element_type=F32
             )
-        y_buf[:, xcol] = jnp.concatenate(parts, axis=1) + spread(skip, g * per, per, width) * xs
+            scores = jnp.where(lower, scores, 0.0)
+            parts = []
+            for j in range(per):
+                h = g * per + j
+                decay = jnp.exp(jnp.minimum(cum[:, h : h + 1] - cum_t[h : h + 1, :], 0.0))
+                parts.append(
+                    jnp.dot((scores * decay).astype(BF16), small_buf[:, h * width : (h + 1) * width],
+                            preferred_element_type=F32)
+                )
+            y_buf[:, xcol] = jnp.concatenate(parts, axis=1) + spread(skip, g * per, per, width) * y_buf[:, xcol]
+
+    @pl.when(zi > 0)
+    def _():
+        inside()
 
     relay(2)
     for i in (3, 4, 5):
-        @pl.when(zi >= i // 2 - i // 4)
+        @pl.when(zi >= i - 2)
         def _():
             relay(i)
 
@@ -331,21 +343,32 @@
                 o_buf.at[other, gl], bef_buf.at[g], o_send.at[gl], o_recv.at[g], (zi * side + other, dp)
             )
         bef_buf[g] = o_buf[yi, gl]
+        if gl in (0, 1):
+            for z in range(1, 4):
+                @pl.when(jnp.minimum(zi, 3) == z)
+                def _():
+                    relay(z + 3 + gl)
+
+    @pl.when(zi == 0)
+    def _():
+        inside()
 
     for i in (12, 13):
         loads[i].wait()
     for i in (3, 4, 5):
-        @pl.when(zi < i // 2 - i // 4)
+        @pl.when(zi == 0)
         def _():
             relay(i)
 
     grow = jnp.exp(cum_buf[...])
     for g in turns:
         xcol = slice(g * wide, (g + 1) * wide)
-        if g == turns[groups // 4]:
-            relay(6)
-        if g == turns[3 * groups // 4]:
-            relay(7)
+        if g in (turns[groups // 4], turns[groups // 2]):
+            i = 6 if g == turns[groups // 4] else 7
+
+            @pl.when(zi < i - 4)
+            def _():
+                relay(i)
 
         @pl.when(g // share != yi)
         def _():
@@ -696,6 +719,7 @@
             halves(ndp, inner // ndp, model), halves(model, shared), halves(model, shared), halves(shared, model),
             halves(model, hidden), halves(model, hidden), halves(hidden, model),
             halves(TAIL, inner), halves(TAIL, span), halves(TAIL, span), floats(tokens, inner), halves(tokens, span),
+            halves(tokens, span), halves(tokens, inner),
             floats(tokens, heads), floats(8, PACK), floats(side, 8, PACK), halves(groups, wide, state),
             halves(side, share, wide, state), halves(share, wide, state), halves(side, share, wide, state),
             halves(share, wide, state), halves(groups, wide, state), halves(tokens, inner),

time: 128 us -> 123 us (0.961)
  Pallas kernels: 126 us -> 120 us
    pallas_call x1, Pallas kernels: 126 us -> 120 us  [body(): pl.pallas_call(lambda *refs: layer_kernel(*refs, depth=depth, side=side,...]
where the time goes in v4:
time: 123 us; the launch traced here: 122 us
  Pallas kernels  120 us (98%)
  local copies, waits for them, and re-layouts  1.88 us (2%)
    pallas_call x1, Pallas kernels, body(): pl.pallas_call(lambda *refs: layer_kernel(*refs, depth=depth, side=side,...  120 us

profile of v4, /device:TPU:17, one launch (start us, length us, event | category | flops | bytes accessed | tf_op | source)
XLA Modules:
  0.0 122.1 jit_solution(2672280662541501242)
XLA Ops:
  0.0 120.2 %shard_map.217 = bf16[128,2048]{1,0:T(8,128)(2,1)} custom-call(bf16[32,128]{1,0:T(8,128)(2,1)} %bitcast.26, s32[2,128]{1,0:T(2,128)} %bitcast.29, f32[2,128]{1,0:T(2,128)} %bitcast.30, f32[1,32]{1,0:T(1,128)} %bitcast.31, f32[1,32]{1,0:T(1,128)} %bitcast.32, f32[1,32]{1,0:T(1,128)} %bitcast.33, bf16[128,2048]{1,0:T(8,128)(2,1)} %bitcast.21, ...), custom_call_target="tpu_custom_call" | custom-call | flops 8000000000 | bytes 24000000 | tf_op jit(solution)/shard_map/pallas_call | solution.py:707
  120.2 1.9 %copy.25 = bf16[1,128,2048]{2,1,0:T(8,128)(2,1)} copy(bf16[1,128,2048]{2,1,0:T(8,128)(2,1)} %bitcast.20) | data formatting | bytes 1048576

commit v5 on v4

--- a/solution.py
+++ b/solution.py
@@ -344,10 +344,15 @@
             )
         bef_buf[g] = o_buf[yi, gl]
         if gl in (0, 1):
-            for z in range(1, 4):
+            for z, i in ((1, 4 + gl), (3, 6 + gl)) + ((2, 6),) * gl:
                 @pl.when(jnp.minimum(zi, 3) == z)
                 def _():
-                    relay(z + 3 + gl)
+                    relay(i)
+
+    @pl.when(zi == 2)
+    def _():
+        relay(5)
+        relay(7)
 
     @pl.when(zi == 0)
     def _():
@@ -366,7 +371,7 @@
         if g in (turns[groups // 4], turns[groups // 2]):
             i = 6 if g == turns[groups // 4] else 7
 
-            @pl.when(zi < i - 4)
+            @pl.when(zi < 2)
             def _():
                 relay(i)
 

time: 123 us -> 121 us (0.984)
  no operation moved by 1% of the time
where the time goes in v5:
time: 121 us
  Pallas kernels  119 us (98%)
  local copies, waits for them, and re-layouts  1.88 us (2%)
    pallas_call x1, Pallas kernels, body(): pl.pallas_call(lambda *refs: layer_kernel(*refs, depth=depth, side=side,...  119 us

profile of v5, /device:TPU:17, one launch (start us, length us, event | category | flops | bytes accessed | tf_op | source)
XLA Modules:
  0.0 121.3 jit_solution(2291033052761904971)
XLA Ops:
  0.0 119.4 %shard_map.217 = bf16[128,2048]{1,0:T(8,128)(2,1)} custom-call(bf16[32,128]{1,0:T(8,128)(2,1)} %bitcast.26, s32[2,128]{1,0:T(2,128)} %bitcast.29, f32[2,128]{1,0:T(2,128)} %bitcast.30, f32[1,32]{1,0:T(1,128)} %bitcast.31, f32[1,32]{1,0:T(1,128)} %bitcast.32, f32[1,32]{1,0:T(1,128)} %bitcast.33, bf16[128,2048]{1,0:T(8,128)(2,1)} %bitcast.21, ...), custom_call_target="tpu_custom_call" | custom-call | flops 8000000000 | bytes 24000000 | tf_op jit(solution)/shard_map/pallas_call | solution.py:712
  119.4 1.9 %copy.25 = bf16[1,128,2048]{2,1,0:T(8,128)(2,1)} copy(bf16[1,128,2048]{2,1,0:T(8,128)(2,1)} %bitcast.20) | data formatting | bytes 1048576
